TPU v7x, 512 devices: a whole 4x8x8 slice. The times are simulated.
512 devices in a mesh: sp: 64 (over z, y), tp: 8 (over x, core).
Axes of the slice: x: 4, y: 8, z: 8, core: 2. Of those that a mesh axis runs over, the one named last changes fastest.
Arguments:
- tokens: bfloat16 [16384, 1024], P(('sp', 'tp')), may hold values from -16 to 16, as said below
- valid_len: int32 [1], replicated, may hold values from 12288 to 16384
- norm_gain: float32 [1024], replicated, may hold values from 0.5 to 1.5
- w_query: bfloat16 [1024, 4096], P(None, 'tp'), may hold values from -0.1875 to 0.1875
- w_key: bfloat16 [1024, 1024], P(None, 'tp'), may hold values from -0.1875 to 0.1875
- w_value: bfloat16 [1024, 1024], P(None, 'tp'), may hold values from -0.1875 to 0.1875
- q_gain: float32 [128], replicated, may hold values from 0.5 to 1.5
- k_gain: float32 [128], replicated, may hold values from 0.5 to 1.5
- w_out: bfloat16 [4096, 1024], P('tp'), may hold values from -0.375 to 0.375
Outputs:
- mixed: bfloat16 [16384, 1024], P(('sp', 'tp'))
Inputs may be any that keep to these rules, and one draw needn't show every extreme that they name: tokens are random entries of unit-order spread (normal or uniform) plus a shift shared by every run of 256 consecutive rows, within -16 and 16. valid_len is at least three quarters of 16384 and at most 16384.
All inputs are finite; a program needn't handle non-finite values.
Results may differ from a plain program's by a relative error of at most 0.02.
Values may be sent and summed in bfloat16 or wider, within the bound.
A program may use at most 64 MiB of HBM per device.

v0:
```python
import jax
import jax.numpy as jnp
from jax import lax
from jax.sharding import PartitionSpec as P

HEAD_DIM = 128
Q_PER_KV = 4
GRID_W = 64


norm_eps = 1e-06
rope_base = 10000.0


def on_whole(section, axis, dim, apply):
    everything = lax.all_gather(section, axis, axis=dim, tiled=True)
    return apply(everything, jnp.int32(0))


def taken_in(value, axis, dim, take_in, carry):
    whole = jax.tree.map(lambda part: lax.all_gather(part, axis, axis=dim, tiled=True), value)
    return take_in(carry, whole, jnp.int32(0))


def shortened(value):
    def short(part):
        return part.astype(jnp.bfloat16) if part.dtype == jnp.float32 else part

    return jax.tree.map(short, value)


def scattered(product, width, axis):
    everything = product(jnp.int32(0), lax.axis_size(axis) * width)
    own = lax.psum_scatter(everything.astype(jnp.bfloat16), axis, scatter_dimension=0, tiled=True)
    return own.astype(jnp.float32)


def normalize(values, gain):
    scaled = values.astype(jnp.float32)
    return scaled * lax.rsqrt(jnp.mean(scaled * scaled, axis=-1, keepdims=True) + norm_eps) * gain


def rope_tables(positions, head_width):
    quarter = head_width // 4
    half_width = head_width // 2
    frequency = rope_base ** (-(jnp.arange(quarter, dtype=jnp.float32) * 2.0) / half_width)
    grid_row = (positions // GRID_W).astype(jnp.float32)
    grid_col = (positions % GRID_W).astype(jnp.float32)
    row_angle = grid_row[:, None] * frequency[None, :]
    col_angle = grid_col[:, None] * frequency[None, :]
    angles = jnp.concatenate([row_angle, row_angle, col_angle, col_angle], axis=-1)
    return (jnp.cos(angles), jnp.sin(angles))


def turn_half(values):
    width = values.shape[-1] // 2
    return jnp.concatenate([-values[..., width:], values[..., :width]], axis=-1)


def prepare(projected, gain, positions, factor):
    head_width = gain.shape[0]
    shaped = projected.astype(jnp.float32).reshape(projected.shape[0], -1, head_width)
    unit = normalize(shaped, gain)
    half_width = head_width // 2
    turned = jnp.concatenate(
        [turn_half(unit[..., :half_width]), turn_half(unit[..., half_width:])], axis=-1
    )
    cosine, sine_table = rope_tables(positions, head_width)
    result = unit * cosine[:, None, :] + turned * sine_table[:, None, :]
    return (result * factor).astype(jnp.bfloat16)


def project_with(weight):

    def apply_weight(pieces, anchor):
        return jnp.dot(pieces, weight, preferred_element_type=jnp.float32).astype(jnp.bfloat16)

    return apply_weight


def on_device(tokens, valid_len, norm_gain, w_query, w_key, w_value, q_gain, k_gain, w_out):
    head_width = q_gain.shape[0]
    local_rows = tokens.shape[0]
    block_rows = local_rows * lax.axis_size("tp")
    normed = normalize(tokens, norm_gain).astype(jnp.bfloat16)
    queries = on_whole(normed, "tp", 0, project_with(w_query))
    keys_all = on_whole(normed, "tp", 0, project_with(w_key))
    values = on_whole(normed, "tp", 0, project_with(w_value))
    offset = lax.axis_index("sp") * block_rows
    positions = offset + jnp.arange(block_rows, dtype=jnp.int32)
    turned_query = prepare(queries, q_gain, positions, HEAD_DIM ** (-0.5))
    turned_key = prepare(keys_all, k_gain, positions, 1.0)
    key_groups = turned_key.shape[1]
    value_heads = values.reshape(block_rows, key_groups, head_width)
    grouped = turned_query.reshape(block_rows, key_groups, Q_PER_KV, head_width).transpose(
        1, 2, 0, 3
    )
    valid = valid_len[0]

    def attend(state_in, key_block, value_block, first_key):
        run_max, totals, accum = state_in
        scores = jnp.einsum(
            "grqd,kgd->grqk", grouped, key_block, preferred_element_type=jnp.float32
        )
        key_pos = first_key + jnp.arange(block_rows, dtype=jnp.int32)
        scores = jnp.where((key_pos < valid)[None, None, None, :], scores, -jnp.inf)
        new_max = jnp.maximum(run_max, jnp.max(scores, axis=-1))
        factor = jnp.exp(run_max - new_max)
        weights = jnp.exp(scores - new_max[..., None])
        totals = totals * factor + jnp.sum(weights, axis=-1)
        update = jnp.einsum(
            "grqk,kgd->grqd",
            weights.astype(jnp.bfloat16),
            value_block,
            preferred_element_type=jnp.float32,
        )
        accum = accum * factor[..., None] + update
        return (new_max, totals, accum)

    def fold_keys(state_now, pieces, anchor):
        key_piece, value_piece = pieces
        shard_count = key_piece.shape[0] // block_rows

        def one_shard(step_index, state_in):
            key_block = lax.dynamic_slice_in_dim(key_piece, step_index * block_rows, block_rows, 0)
            value_block = lax.dynamic_slice_in_dim(
                value_piece, step_index * block_rows, block_rows, 0
            )
            first_key = anchor + step_index * block_rows
            return attend(state_in, key_block, value_block, first_key)

        return lax.fori_loop(0, shard_count, one_shard, state_now)

    stat_shape = (key_groups, Q_PER_KV, block_rows)
    start_state = (
        jnp.full(stat_shape, -1e30, jnp.float32),
        jnp.zeros(stat_shape, jnp.float32),
        jnp.zeros(stat_shape + (head_width,), jnp.float32),
    )
    run_max, totals, accum = taken_in(
        (turned_key, shortened(value_heads)), "sp", 0, fold_keys, start_state
    )
    result = accum / totals[..., None]
    attended = (
        result.transpose(2, 0, 1, 3)
        .reshape(block_rows, key_groups * Q_PER_KV * head_width)
        .astype(jnp.bfloat16)
    )

    def head_terms(anchor, count):
        part_rows = lax.dynamic_slice_in_dim(attended, anchor, count, 0)
        return jnp.dot(part_rows, w_out, preferred_element_type=jnp.float32)

    mixed = scattered(head_terms, local_rows, "tp")
    return mixed.astype(jnp.bfloat16)


def solution(mesh):
    return jax.shard_map(
        on_device,
        mesh=mesh,
        in_specs=(
            P(("sp", "tp"), None),
            P(),
            P(),
            P(None, "tp"),
            P(None, "tp"),
            P(None, "tp"),
            P(),
            P(),
            P("tp", None),
        ),
        out_specs=P(("sp", "tp"), None),
        check_vma=False,
    )
```

profile of v0, /device:TPU:1, one launch (start us, length us, event | category | flops | bytes accessed | tf_op | source)
XLA Modules:
  0.0 468.2 jit_solution(8160096347673318969)
XLA Ops:
  8.6 19.8 %all_gather.11 = bf16[256,1024]{1,0:T(8,128)(2,1)S(1)} all-gather(bf16[32,1024]{1,0:T(8,128)(2,1)S(1)} %fusion.27), channel_id=1, replica_groups=mesh['sp'=64,'tp'=8] {'tp'}, dimensions={0}, use_global_device_ids=true | all-gather | bytes 589824 | tf_op jit(solution)/shard_map/all_gather | solution.py:16
  30.5 1.6 fusion.32
  32.2 1.9 convolution_convert_fusion.2
  35.0 1.7 copy.35
  39.4 77.8 %all-gather.5.cloned.1.call-done = bf16[16384,128]{0,1:T(8,128)(2,1)} async-done(((bf16[256,128]{0,1:T(8,128)(2,1)}), bf16[16384,128]{0,1:T(8,128)(2,1)}) %all-gather.5.cloned.1.call-update) | async-done | bytes 4194320 | tf_op jit(solution)/shard_map/all_gather | solution.py:21
  117.2 85.9 %all-gather.7.cloned.1.call-done = bf16[16384,128]{1,0:T(8,128)(2,1)} async-done(((bf16[256,128]{1,0:T(8,128)(2,1)}), bf16[16384,128]{1,0:T(8,128)(2,1)}) %all-gather.7.cloned.1.call-update) | async-done | bytes 4194320 | tf_op jit(solution)/shard_map/all_gather | solution.py:21
  203.1 220.7 %while.18 = (s32[]{:T(128)}, f32[1,4,256]{2,1,0:T(4,128)S(1)}, f32[1,4,256]{2,1,0:T(4,128)S(1)}, f32[1,4,256,128]{3,2,1,0:T(8,128)S(1)}, s32[]{:T(128)}, /*index...) while((s32[]{:T(128)}, f32[1,4,256]{2,1,0:T(4,128)S(1)}, ...), condition=%wide.region_6.7_spmd.clone, body=%wide.region_3.6_spmd.clone.sunk | while | flops 136190464 | bytes 4653759 | solution.py:132
  205.0 1.4 fusion.59
  208.4 1.4 fusion.59
  211.9 1.4 fusion.59
  215.3 1.4 fusion.59
  218.8 1.4 fusion.59
  222.2 1.4 fusion.59
  225.7 1.4 fusion.59
  229.1 1.4 fusion.59
  232.6 1.4 fusion.59
  236.0 1.4 fusion.59
  239.5 1.4 fusion.59
  242.9 1.4 fusion.59
  246.4 1.4 fusion.59
  249.8 1.4 fusion.59
  253.2 1.4 fusion.59
  256.7 1.4 fusion.59
  260.1 1.4 fusion.59
  263.6 1.4 fusion.59
  267.0 1.4 fusion.59
  270.5 1.4 fusion.59
  273.9 1.4 fusion.59
  277.4 1.4 fusion.59
  280.8 1.4 fusion.59
  284.3 1.4 fusion.59
  287.7 1.4 fusion.59
  294.6 1.4 fusion.59
  298.1 1.4 fusion.59
  301.5 1.4 fusion.59
  305.0 1.4 fusion.59
  308.4 1.4 fusion.59
  311.9 1.4 fusion.59
  318.8 1.4 fusion.59
  322.2 1.4 fusion.59
  325.7 1.4 fusion.59
  332.6 1.4 fusion.59
  336.0 1.4 fusion.59
  339.5 1.4 fusion.59
  342.9 1.4 fusion.59
  349.8 1.4 fusion.59
  353.3 1.4 fusion.59
  356.7 1.4 fusion.59
  360.2 1.4 fusion.59
  363.6 1.4 fusion.59
  367.0 1.4 fusion.59
  370.5 1.4 fusion.59
  373.9 1.4 fusion.59
  377.4 1.4 fusion.59
  380.8 1.4 fusion.59
  387.7 1.4 fusion.59
  391.2 1.4 fusion.59
  394.6 1.4 fusion.59
  405.0 1.4 fusion.59
  408.4 1.4 fusion.59
  411.9 1.4 fusion.59
  418.8 1.4 fusion.59
  422.2 1.4 fusion.59
  425.4 36.3 %reduce-scatter.2.cloned.1.call-done = bf16[32,1024]{1,0:T(8,128)(2,1)} async-done(((bf16[256,1024]{1,0:T(8,128)(2,1)}), bf16[32,1024]{1,0:T(8,128)(2,1)}) %reduce-scatter.2.cloned.1.call-update) | async-done | bytes 65552 | tf_op jit(solution)/shard_map/reduce_scatter | solution.py:34
  (434 shorter events, 149.9 us)
Async XLA Ops:
  6.5 417.5 %copy-start = (bf16[512,1024]{1,0:T(8,128)(2,1)S(1)}, bf16[512,1024]{1,0:T(8,128)(2,1)}, u32[]{:S(2)}) copy-start(bf16[512,1024]{1,0:T(8,128)(2,1)} %param.19) | copy-start | bytes 3145732
  6.5 27.6 %copy-start.1 = (bf16[1024,512]{1,0:T(8,128)(2,1)S(1)}, bf16[1024,512]{1,0:T(8,128)(2,1)}, u32[]{:S(2)}) copy-start(bf16[1024,512]{1,0:T(8,128)(2,1)} %param.14) | copy-start | bytes 3145732
  6.5 110.6 %all-gather.5.cloned.1.call-start = ((), (), s32[]{:S(2)}) async-start(), calls=%async_computation.2 | async-start | bytes 4259840 | tf_op jit(solution)/shard_map/all_gather | solution.py:21
  28.4 9.5 %copy-start.4 = (f32[128]{0:T(128)S(1)}, f32[128]{0:T(128)}, u32[]{:S(2)}) copy-start(f32[128]{0:T(128)} %param.17) | copy-start | bytes 1540
  32.2 170.9 %all-gather.7.cloned.1.call-start = ((), (), s32[]{:S(2)}) async-start(), calls=%async_computation.3 | async-start | bytes 4259840 | tf_op jit(solution)/shard_map/all_gather | solution.py:21
  34.1 427.6 %reduce-scatter.2.cloned.1.call-start = ((), (), s32[]{:S(2)}) async-start(), calls=%async_computation.1 | async-start | bytes 589824 | tf_op jit(solution)/shard_map/reduce_scatter | solution.py:34
  37.4 1.1 copy-start.2
  37.8 0.9 copy-start.3
Sparse Core Ops, SparseCore 0:
  32.3 84.8 all-gather.4
  120.2 82.8 all-gather.6
  425.5 36.1 reduce-scatter.1
where the time goes:
time: 475 us; the launch traced here: 468 us
  waiting for transfers between devices  200 us (42%)
  matrix products  168 us (35%)
  other arithmetic  60.2 us (13%)
  blocking collectives  19.8 us (4%)
  between operations  13.3 us (3%)
    all_gather x2, waiting for transfers between devices, taken_in(): lax.all_gather(part, axis, axis=dim, tiled=True)  164 us
    dot_general x64, matrix products, attend(): jnp.einsum('grqk,kgd->grqd', weights.astype(jnp.bfloat16), value_block, p...  87.2 us
    dot_general x64, matrix products, attend(): jnp.einsum('grqd,kgd->grqk', grouped, key_block, preferred_element_type=j...  75.5 us
    lt x64, other arithmetic, attend(): scores = jnp.where((key_pos < valid)[None, None, None, :], scores, -jnp.inf)  41.8 us
    reduce_scatter x1, waiting for transfers between devices, scattered(): lax.psum_scatter(everything.astype(jnp.bfloat16), axis, scatter_dimension...  36.3 us
    all_gather x1, blocking collectives, on_whole(): everything = lax.all_gather(section, axis, axis=dim, tiled=True)  19.8 us
    reduce_sum x64, other arithmetic, attend(): totals = totals * factor + jnp.sum(weights, axis=-1)  10.4 us
  transfers between devices with their start and end apart: 3, of which 3 were waited for; matrix products, arithmetic and copies ran while one was open for 1% of the time, Pallas kernels for 0%

commit v1 on v0

v1 whole, which is shorter than its diff:
```python
import functools
import math

import jax
import jax.numpy as jnp
import numpy as np
from jax import lax
from jax.experimental import pallas as pl
from jax.experimental.pallas import tpu as pltpu
from jax.sharding import PartitionSpec as P

HEAD_DIM = 128
Q_PER_KV = 4
GRID_W = 64
RING = 8
N_TP = 8
ROWS = 32
BLOCK = 256
HALF = 128
EPS = 1e-06
MESH = pl.DeviceIdType.MESH
OFFSETS = (0, -1, 1, -2, 2, -3, 3, -4)
Q_SCALE = HEAD_DIM ** -0.5 * math.log2(math.e)


def rope_constants():
    freq = np.float32(10000.0) ** (-(np.arange(32, dtype=np.float32) * 2.0) / 64)
    freq = freq.astype(np.float32)
    sign = np.concatenate([-np.ones(32), np.ones(32)]).astype(np.float32)

    def table(count):
        angle = (np.arange(count, dtype=np.float32)[:, None] * freq[None, :]).astype(np.float64)
        angle = np.concatenate([angle, angle], axis=1)
        return np.cos(angle).astype(np.float32), np.sin(angle).astype(np.float32) * sign

    row_cos, row_sin = table(256)
    col_cos, col_sin = table(64)
    rows = np.zeros((64, 8, 128), np.float32)
    rows[:, 0:4, 0:64] = row_cos.reshape(64, 4, 64)
    rows[:, 4:8, 0:64] = row_sin.reshape(64, 4, 64)
    cols = np.zeros((2, 64, 128), np.float32)
    cols[0, :, 64:] = col_cos
    cols[1, :, 64:] = col_sin
    return rows, cols


def kernel(tok, valid, ngain, wq_hbm, wk_hbm, wv_hbm, qgain, kgain, wo_hbm, rowtab_hbm, coltab,
           out, x, wq, wk, wv, wo, rowtab, cosv, sinv, kv, qs, mask, acc, lsum, att, part, rs,
           w_sem, xs_sem, xr_sem, s1_sem, r1_sem, s2_sem, r2_sem, os_sem, or_sem):
    sp = lax.axis_index("sp")
    tp = lax.axis_index("tp")
    z = sp // RING
    y = sp % RING

    def wrap(a):
        return lax.rem(a + 2 * RING, RING)

    def at(zz, yy):
        return {"sp": zz * RING + yy, "tp": tp}

    up = {"y": (at(z, wrap(y + 1)), at(z, wrap(y - 1))), "z": (at(wrap(z + 1), y), at(wrap(z - 1), y))}
    first = ("y", "z")
    second = ("z", "y")
    peers = [{"sp": sp, "tp": lax.rem(tp + k, N_TP)} for k in range(1, N_TP)]

    loads = [
        pltpu.make_async_copy(wk_hbm, wk, w_sem.at[0]),
        pltpu.make_async_copy(wv_hbm, wv, w_sem.at[1]),
        pltpu.make_async_copy(rowtab_hbm.at[sp], rowtab, w_sem.at[2]),
        pltpu.make_async_copy(wq_hbm, wq, w_sem.at[3]),
        pltpu.make_async_copy(wo_hbm, wo, w_sem.at[4]),
    ]
    for load in loads:
        load.start()

    barrier = pltpu.get_barrier_semaphore()
    everyone = peers + [up["y"][0], up["y"][1], up["z"][0], up["z"][1]]
    for peer in everyone:
        pl.semaphore_signal(barrier, inc=1, device_id=peer, device_id_type=MESH)

    scaled = tok[...].astype(jnp.float32)
    inv = lax.rsqrt(jnp.mean(scaled * scaled, axis=-1, keepdims=True) + EPS)
    x[tp] = (scaled * inv * ngain[...]).astype(jnp.bfloat16)
    acc[...] = jnp.zeros_like(acc)
    lsum[...] = jnp.zeros_like(lsum)

    pl.semaphore_wait(barrier, len(everyone))

    def xcopy(k):
        return pltpu.make_async_remote_copy(
            src_ref=x.at[tp], dst_ref=x.at[tp], send_sem=xs_sem.at[k], recv_sem=xr_sem.at[k],
            device_id=peers[k], device_id_type=MESH)

    for k in range(N_TP - 1):
        xcopy(k).start()

    loads[2].wait()
    for r in range(4):
        cosv[r * 64:(r + 1) * 64, :] = rowtab[r:r + 1, :] + coltab[0]
        sinv[r * 64:(r + 1) * 64, :] = rowtab[4 + r:5 + r, :] + coltab[1]

    limit = valid[0]
    lane = lax.broadcasted_iota(jnp.int32, (1, HALF), 1)

    def mask_row(slot, block, half):
        pos = block * BLOCK + half * HALF + lane
        mask[slot] = jnp.broadcast_to((pos < limit).astype(jnp.float32), (8, HALF))

    for part_id in range(2):
        for p in range(8):
            def source(dist, p=p, part_id=part_id):
                if part_id == 0:
                    return wrap(z + dist) * RING + wrap(y + OFFSETS[p])
                return wrap(z + OFFSETS[p]) * RING + wrap(y + dist)
            mask_row(part_id * 64 + p, source(0), part_id)
            sub, q = p // 4, p % 4
            for dist in range(1, 4):
                j = (dist - 1) * 2 + sub
                mask_row(part_id * 64 + 8 + 4 * j + q, source(-dist), part_id)
                mask_row(part_id * 64 + 36 + 4 * j + q, source(dist), part_id)
            mask_row(part_id * 64 + (8 if sub == 0 else 36) + 24 + q, source(-4), part_id)

    loads[0].wait()
    loads[1].wait()
    for k in range(N_TP - 1):
        xcopy(k).wait_recv()

    everything = x[...].reshape(BLOCK, x.shape[2])
    cosine = cosv[...]
    sine = sinv[...]
    in_first = (lax.broadcasted_iota(jnp.int32, (BLOCK, HEAD_DIM), 1) % 64) < 32

    def turn(projected, gain, factor):
        v = projected.astype(jnp.bfloat16).astype(jnp.float32)
        u = v * lax.rsqrt(jnp.mean(v * v, axis=-1, keepdims=True) + EPS) * gain
        moved = jnp.where(in_first, pltpu.roll(u, 96, 1), pltpu.roll(u, 32, 1))
        return (u * cosine + moved * sine) * factor

    keys = turn(jnp.dot(everything, wk[...], preferred_element_type=jnp.float32), kgain[...], 1.0)
    rows = sp * BLOCK + lax.broadcasted_iota(jnp.int32, (BLOCK, HEAD_DIM), 0)
    vals = jnp.dot(everything, wv[...], preferred_element_type=jnp.float32)
    vals = jnp.where(rows < limit, vals, 0.0).astype(jnp.bfloat16)
    for part_id in range(2):
        piece = slice(part_id * HALF, (part_id + 1) * HALF)
        kv[part_id * 64, 0:HALF, :] = keys[piece, :].T.astype(jnp.bfloat16)
        kv[part_id * 64, HALF:, :] = vals[piece, :]

    def hop(part_id, h, d):
        if d == 0:
            src, dst = (0 if h == 1 else 2 * h - 3), 2 * h - 1
        else:
            src, dst = (0 if h == 1 else 2 * h - 2), 2 * h
        return pltpu.make_async_remote_copy(
            src_ref=kv.at[part_id * 64 + src], dst_ref=kv.at[part_id * 64 + dst],
            send_sem=s1_sem.at[part_id, d, h - 1], recv_sem=r1_sem.at[part_id, d, h - 1],
            device_id=up[first[part_id]][d], device_id_type=MESH)

    def place(part_id, d, j):
        return part_id * 64 + 8 + 28 * d + 4 * j

    def hand_on(part_id, d, p):
        return pltpu.make_async_remote_copy(
            src_ref=kv.at[part_id * 64 + p], dst_ref=kv.at[place(part_id, d, p // 4) + p % 4],
            send_sem=s2_sem.at[part_id, d, p // 4], recv_sem=r2_sem.at[part_id, d, p // 4],
            device_id=up[second[part_id]][d], device_id_type=MESH)

    def relay(part_id, d, j, to):
        return pltpu.make_async_remote_copy(
            src_ref=kv.at[pl.ds(place(part_id, d, j), 4)], dst_ref=kv.at[pl.ds(place(part_id, d, to), 4)],
            send_sem=s2_sem.at[part_id, d, to], recv_sem=r2_sem.at[part_id, d, to],
            device_id=up[second[part_id]][d], device_id_type=MESH)

    both = [(a, d) for a in range(2) for d in range(2)]
    for a, d in both:
        hop(a, 1, d).start()
    for a, d in both:
        hand_on(a, d, 0).start()

    loads[3].wait()
    for h in range(Q_PER_KV):
        query = jnp.dot(everything, wq[:, h * HEAD_DIM:(h + 1) * HEAD_DIM], preferred_element_type=jnp.float32)
        qs[h * BLOCK:(h + 1) * BLOCK, :] = turn(query, qgain[...], Q_SCALE).astype(jnp.bfloat16)

    def attend(base0, base1):
        slots = [base0 + i for i in range(4)] + [base1 + i for i in range(4)]
        kt = jnp.concatenate([kv[s, 0:HALF, :] for s in slots], axis=1)
        v = jnp.concatenate([kv[s, HALF:, :] for s in slots], axis=0)
        marks = [mask[s, 0:1, :] for s in slots]
        for r in range(2):
            span = pl.ds(r * 512, 512)
            s = jnp.dot(qs[span, :], kt, preferred_element_type=jnp.float32)
            w = jnp.exp2(s)
            acc[span, :] += jnp.dot(w.astype(jnp.bfloat16), v, preferred_element_type=jnp.float32)
            t = w[:, 0:HALF] * marks[0]
            for i in range(1, 8):
                t = t + w[:, i * HALF:(i + 1) * HALF] * marks[i]
            lsum[span, :] += t

    def first_step(h):
        ways = (0, 1) if h < 4 else (0,)
        for a in range(2):
            for d in ways:
                hop(a, h, d).wait_recv()
                if h + 1 < 4 or (h + 1 == 4 and d == 0):
                    hop(a, h + 1, d).start()
        for a in range(2):
            for d in ways:
                for e in range(2):
                    hand_on(a, e, 2 * h - 1 + d).start()

    for h in (1, 2, 3):
        first_step(h)
    for a, d in both:
        relay(a, d, 0, 0).wait_recv()
        relay(a, d, 0, 2).start()
    first_step(4)

    def own(a, c):
        attend(a * 64, a * 64 + 4)
        return c

    lax.fori_loop(0, 2, own, 0)

    def step(j, c):
        for a in range(2):
            for d in range(2):
                @pl.when(j > 0)
                def _():
                    relay(a, d, j, j).wait_recv()

                    @pl.when(j < (5 if d == 0 else 4))
                    def _():
                        relay(a, d, j, j + 2).start()
                    if d == 1:
                        @pl.when(j == 5)
                        def _():
                            relay(a, d, j, j + 1).start()
            attend(place(a, 0, j), place(a, 1, j))
        return c

    lax.fori_loop(0, 7, step, 0)

    loads[4].wait()
    for h in range(Q_PER_KV):
        span = slice(h * BLOCK, (h + 1) * BLOCK)
        total = jnp.sum(lsum[span, :], axis=-1, keepdims=True)
        att[:, h * HEAD_DIM:(h + 1) * HEAD_DIM] = (acc[span, :] / total).astype(jnp.bfloat16)
    mixed = jnp.dot(att[...], wo[...], preferred_element_type=jnp.float32)
    part[...] = mixed.astype(jnp.bfloat16).reshape(part.shape)

    def ocopy(k):
        return pltpu.make_async_remote_copy(
            src_ref=part.at[lax.rem(tp + k + 1, N_TP)], dst_ref=rs.at[k], send_sem=os_sem.at[k],
            recv_sem=or_sem.at[k], device_id=peers[k], device_id_type=MESH)

    for k in range(N_TP - 1):
        ocopy(k).start()

    for k in range(N_TP - 1):
        xcopy(k).wait_send()
    for a, d in both:
        for h in range(1, 5 - d):
            hop(a, h, d).wait_send()
        for j in range(7):
            relay(a, d, 0, j).wait_send()

    total = part[tp].astype(jnp.float32)
    for k in range(N_TP - 1):
        ocopy(k).wait_recv()
        total = total + rs[k].astype(jnp.float32)
    out[...] = total.astype(jnp.bfloat16)
    for k in range(N_TP - 1):
        ocopy(k).wait_send()


def on_device(tokens, valid_len, norm_gain, w_query, w_key, w_value, q_gain, k_gain, w_out):
    rows, cols = rope_constants()
    width = tokens.shape[1]
    vmem = pl.BlockSpec(memory_space=pltpu.VMEM)
    anywhere = pl.BlockSpec(memory_space=pl.ANY)
    dma = pltpu.SemaphoreType.DMA
    call = pl.pallas_call(
        kernel,
        out_shape=jax.ShapeDtypeStruct(tokens.shape, jnp.bfloat16),
        in_specs=[vmem, pl.BlockSpec(memory_space=pltpu.SMEM), vmem, anywhere, anywhere, anywhere,
                  vmem, vmem, anywhere, anywhere, vmem],
        out_specs=vmem,
        scratch_shapes=[
            pltpu.VMEM((N_TP, ROWS, width), jnp.bfloat16),
            pltpu.VMEM(w_query.shape, jnp.bfloat16),
            pltpu.VMEM(w_key.shape, jnp.bfloat16),
            pltpu.VMEM(w_value.shape, jnp.bfloat16),
            pltpu.VMEM(w_out.shape, jnp.bfloat16),
            pltpu.VMEM((8, HEAD_DIM), jnp.float32),
            pltpu.VMEM((BLOCK, HEAD_DIM), jnp.float32),
            pltpu.VMEM((BLOCK, HEAD_DIM), jnp.float32),
            pltpu.VMEM((128, 2 * HALF, HEAD_DIM), jnp.bfloat16),
            pltpu.VMEM((Q_PER_KV * BLOCK, HEAD_DIM), jnp.bfloat16),
            pltpu.VMEM((128, 8, HALF), jnp.float32),
            pltpu.VMEM((Q_PER_KV * BLOCK, HEAD_DIM), jnp.float32),
            pltpu.VMEM((Q_PER_KV * BLOCK, HEAD_DIM), jnp.float32),
            pltpu.VMEM((BLOCK, Q_PER_KV * HEAD_DIM), jnp.bfloat16),
            pltpu.VMEM((N_TP, ROWS, width), jnp.bfloat16),
            pltpu.VMEM((N_TP - 1, ROWS, width), jnp.bfloat16),
            dma((5,)), dma((7,)), dma((7,)), dma((2, 2, 4)), dma((2, 2, 4)), dma((2, 2, 7)), dma((2, 2, 7)),
            dma((7,)), dma((7,)),
        ],
        compiler_params=pltpu.CompilerParams(
            collective_id=0, has_side_effects=True, vmem_limit_bytes=48 * 2 ** 20),
        name="fused_attention",
    )
    return call(tokens, valid_len, norm_gain.reshape(1, -1), w_query, w_key, w_value,
                q_gain.reshape(1, -1), k_gain.reshape(1, -1), w_out, jnp.asarray(rows), jnp.asarray(cols))


def solution(mesh):
    return jax.shard_map(
        on_device,
        mesh=mesh,
        in_specs=(
            P(("sp", "tp"), None),
            P(),
            P(),
            P(None, "tp"),
            P(None, "tp"),
            P(None, "tp"),
            P(),
            P(),
            P("tp", None),
        ),
        out_specs=P(("sp", "tp"), None),
        check_vma=False,
    )
```

time: 475 us -> 94.8 us (0.20); the launches traced: 468 us -> 93.6 us
  waiting for transfers between devices: 200 us -> 0 us
  matrix products: 168 us -> 0 us
  Pallas kernels: 0 us -> 84.6 us
  other arithmetic: 60.2 us -> 0 us
  blocking collectives: 19.8 us -> 0 us
  between operations: 13.3 us -> 0.71 us
  local copies, waits for them, and re-layouts: 3.43 us -> 8.26 us
    dot_general x132 -> x0, matrix products: 168 us -> none  [the longest x64 87.2 us: attend(): jnp.einsum('grqk,kgd->grqd', weights.astype(jnp.bfloat16), value_block, p...]
    all_gather x2 -> x0, waiting for transfers between devices: 164 us -> none  [taken_in(): lax.all_gather(part, axis, axis=dim, tiled=True)]
    pallas_call x0 -> x1, Pallas kernels: none -> 84.6 us  [on_device(): call(tokens, valid_len, norm_gain.reshape(1, -1), w_query, w_key, w_value...]
    lt x64 -> x0, other arithmetic: 41.8 us -> none  [attend(): scores = jnp.where((key_pos < valid)[None, None, None, :], scores, -jnp.inf)]
    reduce_scatter x1 -> x0, waiting for transfers between devices: 36.3 us -> none  [scattered(): lax.psum_scatter(everything.astype(jnp.bfloat16), axis, scatter_dimension...]
    all_gather x1 -> x0, blocking collectives: 19.8 us -> none  [on_whole(): everything = lax.all_gather(section, axis, axis=dim, tiled=True)]
    reduce_sum x66 -> x0, other arithmetic: 11.8 us -> none  [the longest x64 10.4 us: attend(): totals = totals * factor + jnp.sum(weights, axis=-1)]
    unnamed x10 -> x21, local copies, waits for them, and re-layouts: 0.23 us -> 8.26 us
  transfers between devices with their start and end apart: 3 -> 0, of which waited for: 3 -> 0; matrix products, arithmetic and copies ran while one was open for 1% -> 0% of each run, Pallas kernels for 0% -> 0%
where the time goes in v1:
time: 94.8 us; the launch traced here: 93.6 us
  Pallas kernels  84.6 us (89%)
  local copies, waits for them, and re-layouts  8.26 us (9%)
    pallas_call x1, Pallas kernels, on_device(): call(tokens, valid_len, norm_gain.reshape(1, -1), w_query, w_key, w_value...  84.6 us
    unnamed x21, local copies, waits for them, and re-layouts  8.26 us

profile of v1, /device:TPU:1, one launch (start us, length us, event | category | flops | bytes accessed | tf_op | source)
XLA Modules:
  0.0 93.6 jit_solution(6913743391742924440)
XLA Ops:
  0.0 0.0 copy-start.7
  0.7 0.0 copy-start.8
  0.7 0.0 copy-start.9
  0.7 0.0 copy-done.7
  0.7 0.6 copy-done.8
  1.3 0.0 copy-done.9
  1.3 0.0 copy-start
  1.3 1.2 %copy-done = bf16[1024,512]{1,0:T(8,128)(2,1)S(1)} copy-done((bf16[1024,512]{1,0:T(8,128)(2,1)S(1)}, bf16[1024,512]{1,0:T(8,128)(2,1)}, u32[]{:S(2)}) %copy-start) | copy-done | bytes 1048600
  2.6 0.0 copy-start.1
  2.6 1.2 %copy-done.1 = bf16[512,1024]{1,0:T(8,128)(2,1)S(1)} copy-done((bf16[512,1024]{1,0:T(8,128)(2,1)S(1)}, bf16[512,1024]{1,0:T(8,128)(2,1)}, u32[]{:S(2)}) %copy-start.1) | copy-done | bytes 1048600
  3.8 0.0 copy-start.2
  3.8 0.9 %copy-done.2 = bf16[1024,128]{1,0:T(8,128)(2,1)S(1)} copy-done((bf16[1024,128]{1,0:T(8,128)(2,1)S(1)}, bf16[1024,128]{1,0:T(8,128)(2,1)}, u32[]{:S(2)}) %copy-start.2) | copy-done | bytes 262168
  4.7 0.0 copy-start.3
  4.7 0.9 %copy-done.3 = bf16[1024,128]{1,0:T(8,128)(2,1)S(1)} copy-done((bf16[1024,128]{1,0:T(8,128)(2,1)S(1)}, bf16[1024,128]{1,0:T(8,128)(2,1)}, u32[]{:S(2)}) %copy-start.3) | copy-done | bytes 262168
  5.7 0.0 copy-start.4
  5.7 0.9 %copy-done.4 = f32[64,8,128]{2,1,0:T(8,128)S(1)} copy-done((f32[64,8,128]{2,1,0:T(8,128)S(1)}, f32[64,8,128]{2,1,0:T(8,128)}, u32[]{:S(2)}) %copy-start.4) | copy-done | bytes 262168
  6.6 0.0 copy-start.5
  6.6 0.8 copy-done.5
  7.5 0.0 copy-start.6
  7.5 0.8 copy-done.6
  8.3 84.6 %fused_attention.1 = bf16[32,1024]{1,0:T(8,128)(2,1)S(1)} custom-call(bf16[32,1024]{1,0:T(8,128)(2,1)S(1)} %copy-done.5, s32[1]{0:T(128)S(6)} %copy.13.valid, f32[1,1024]{1,0:T(1,128)S(1)} %bitcast.3, bf16[1024,512]{1,0:T(8,128)(2,1)S(1)} %copy-done, bf16[1024,128]{1,0:T(8,128)(2,1)S(1)} %copy-done.2, bf16[1024,128]{1,0:T(8,128)(2,1)S(1)} %copy-done.3, ...), custom_call_target="tpu_custom_call" | custom-call | tf_op jit(solution)/shard_map/fused_attention/pallas_call | solution.py:312
  93.0 0.6 copy.14
Async XLA Ops:
  0.0 0.7 copy-start.7
  0.7 0.7 copy-start.8
  0.7 0.7 copy-start.9
  1.3 1.2 %copy-start = (bf16[1024,512]{1,0:T(8,128)(2,1)S(1)}, bf16[1024,512]{1,0:T(8,128)(2,1)}, u32[]{:S(2)}) copy-start(bf16[1024,512]{1,0:T(8,128)(2,1)} %wq_hbm.1) | copy-start | bytes 3145732
  2.6 1.2 %copy-start.1 = (bf16[512,1024]{1,0:T(8,128)(2,1)S(1)}, bf16[512,1024]{1,0:T(8,128)(2,1)}, u32[]{:S(2)}) copy-start(bf16[512,1024]{1,0:T(8,128)(2,1)} %wo_hbm.1) | copy-start | bytes 3145732
  3.8 0.9 %copy-start.2 = (bf16[1024,128]{1,0:T(8,128)(2,1)S(1)}, bf16[1024,128]{1,0:T(8,128)(2,1)}, u32[]{:S(2)}) copy-start(bf16[1024,128]{1,0:T(8,128)(2,1)} %wk_hbm.1) | copy-start | bytes 786436
  4.7 0.9 %copy-start.3 = (bf16[1024,128]{1,0:T(8,128)(2,1)S(1)}, bf16[1024,128]{1,0:T(8,128)(2,1)}, u32[]{:S(2)}) copy-start(bf16[1024,128]{1,0:T(8,128)(2,1)} %wv_hbm.1) | copy-start | bytes 786436
  5.7 0.9 %copy-start.4 = (f32[64,8,128]{2,1,0:T(8,128)S(1)}, f32[64,8,128]{2,1,0:T(8,128)}, u32[]{:S(2)}) copy-start(f32[64,8,128]{2,1,0:T(8,128)} %constant.4.clone.rowtab_hbm) | copy-start | bytes 786436
  6.6 0.8 copy-start.5
  7.5 0.8 copy-start.6

commit v2 on v1

--- a/solution.py
+++ b/solution.py
@@ -14,6 +14,7 @@
 GRID_W = 64
 RING = 8
 N_TP = 8
+N_X = 4
 ROWS = 32
 BLOCK = 256
 HALF = 128
@@ -44,9 +45,9 @@
     return rows, cols
 
 
-def kernel(tok, valid, ngain, wq_hbm, wk_hbm, wv_hbm, qgain, kgain, wo_hbm, rowtab_hbm, coltab,
-           out, x, wq, wk, wv, wo, rowtab, cosv, sinv, kv, qs, mask, acc, lsum, att, part, rs,
-           w_sem, xs_sem, xr_sem, s1_sem, r1_sem, s2_sem, r2_sem, os_sem, or_sem):
+def kernel(tok_hbm, valid, ngain_hbm, wq_hbm, wk_hbm, wv_hbm, qgain_hbm, kgain_hbm, wo_hbm, rowtab_hbm, coltab_hbm,
+           out, tok, ngain, qgain, kgain, coltab, x, wq, wk, wv, wo, rowtab, cosv, sinv, kv, qs, mask, acc, lsum, att, partial, to_twin, from_twin, summed, arrived,
+           w_sem, xs_sem, xr_sem, s1_sem, r1_sem, s2_sem, r2_sem, ds_sem, dr_sem, os_sem, or_sem):
     sp = lax.axis_index("sp")
     tp = lax.axis_index("tp")
     z = sp // RING
@@ -61,7 +62,10 @@
     up = {"y": (at(z, wrap(y + 1)), at(z, wrap(y - 1))), "z": (at(wrap(z + 1), y), at(wrap(z - 1), y))}
     first = ("y", "z")
     second = ("z", "y")
-    peers = [{"sp": sp, "tp": lax.rem(tp + k, N_TP)} for k in range(1, N_TP)]
+    core = lax.rem(tp, 2)
+    column = tp // 2
+    twin = {"sp": sp, "tp": tp + 1 - 2 * core}
+    peers = [{"sp": sp, "tp": lax.rem(tp + 2 * k, N_TP)} for k in range(1, N_X)]
 
     loads = [
         pltpu.make_async_copy(wk_hbm, wk, w_sem.at[0]),
@@ -69,15 +73,26 @@
         pltpu.make_async_copy(rowtab_hbm.at[sp], rowtab, w_sem.at[2]),
         pltpu.make_async_copy(wq_hbm, wq, w_sem.at[3]),
         pltpu.make_async_copy(wo_hbm, wo, w_sem.at[4]),
+        pltpu.make_async_copy(coltab_hbm, coltab, w_sem.at[5]),
+        pltpu.make_async_copy(qgain_hbm, qgain, w_sem.at[6]),
+        pltpu.make_async_copy(kgain_hbm, kgain, w_sem.at[7]),
     ]
+    early = [
+        pltpu.make_async_copy(tok_hbm, tok, w_sem.at[8]),
+        pltpu.make_async_copy(ngain_hbm, ngain, w_sem.at[9]),
+    ]
+    for load in early:
+        load.start()
     for load in loads:
         load.start()
 
     barrier = pltpu.get_barrier_semaphore()
-    everyone = peers + [up["y"][0], up["y"][1], up["z"][0], up["z"][1]]
+    everyone = peers + [twin, up["y"][0], up["y"][1], up["z"][0], up["z"][1]]
     for peer in everyone:
         pl.semaphore_signal(barrier, inc=1, device_id=peer, device_id_type=MESH)
 
+    for load in early:
+        load.wait()
     scaled = tok[...].astype(jnp.float32)
     inv = lax.rsqrt(jnp.mean(scaled * scaled, axis=-1, keepdims=True) + EPS)
     x[tp] = (scaled * inv * ngain[...]).astype(jnp.bfloat16)
@@ -86,15 +101,17 @@
 
     pl.semaphore_wait(barrier, len(everyone))
 
-    def xcopy(k):
-        return pltpu.make_async_remote_copy(
-            src_ref=x.at[tp], dst_ref=x.at[tp], send_sem=xs_sem.at[k], recv_sem=xr_sem.at[k],
-            device_id=peers[k], device_id_type=MESH)
-
-    for k in range(N_TP - 1):
-        xcopy(k).start()
-
-    loads[2].wait()
+    def xcopy(i):
+        slot = tp if i < N_X else lax.rem(tp + 2 * N_TP - 2 * (i - N_X + 1), N_TP)
+        return pltpu.make_async_remote_copy(
+            src_ref=x.at[slot], dst_ref=x.at[slot], send_sem=xs_sem.at[i], recv_sem=xr_sem.at[i],
+            device_id=peers[i - 1] if 0 < i < N_X else twin, device_id_type=MESH)
+
+    for i in (2, 1, 3, 0):
+        xcopy(i).start()
+
+    for i in (2, 5, 6, 7):
+        loads[i].wait()
     for r in range(4):
         cosv[r * 64:(r + 1) * 64, :] = rowtab[r:r + 1, :] + coltab[0]
         sinv[r * 64:(r + 1) * 64, :] = rowtab[4 + r:5 + r, :] + coltab[1]
@@ -122,8 +139,11 @@
 
     loads[0].wait()
     loads[1].wait()
-    for k in range(N_TP - 1):
+    for k in (1, 3, 2):
         xcopy(k).wait_recv()
+        xcopy(k + N_X - 1).start()
+    for i in (0, 4, 6, 5):
+        xcopy(i).wait_recv()
 
     everything = x[...].reshape(BLOCK, x.shape[2])
     cosine = cosv[...]
@@ -170,6 +190,13 @@
             send_sem=s2_sem.at[part_id, d, to], recv_sem=r2_sem.at[part_id, d, to],
             device_id=up[second[part_id]][d], device_id_type=MESH)
 
+    def last(part_id, d, i):
+        return pltpu.make_async_remote_copy(
+            src_ref=kv.at[pl.ds(place(part_id, d, 4 + d) + 2 * i, 2)],
+            dst_ref=kv.at[pl.ds(place(part_id, d, 6) + 2 * i, 2)],
+            send_sem=s2_sem.at[part_id, d, 6 + i], recv_sem=r2_sem.at[part_id, d, 6 + i],
+            device_id=up[second[part_id]][d], device_id_type=MESH)
+
     both = [(a, d) for a in range(2) for d in range(2)]
     for a, d in both:
         hop(a, 1, d).start()
@@ -179,14 +206,15 @@
     loads[3].wait()
     for h in range(Q_PER_KV):
         query = jnp.dot(everything, wq[:, h * HEAD_DIM:(h + 1) * HEAD_DIM], preferred_element_type=jnp.float32)
-        qs[h * BLOCK:(h + 1) * BLOCK, :] = turn(query, qgain[...], Q_SCALE).astype(jnp.bfloat16)
-
-    def attend(base0, base1):
-        slots = [base0 + i for i in range(4)] + [base1 + i for i in range(4)]
+        query = turn(query, qgain[...], Q_SCALE).astype(jnp.bfloat16)
+        for r in range(2):
+            qs[r * 512 + h * HALF:r * 512 + (h + 1) * HALF, :] = query[r * HALF:(r + 1) * HALF, :]
+
+    def attend(slots, rows):
         kt = jnp.concatenate([kv[s, 0:HALF, :] for s in slots], axis=1)
         v = jnp.concatenate([kv[s, HALF:, :] for s in slots], axis=0)
         marks = [mask[s, 0:1, :] for s in slots]
-        for r in range(2):
+        for r in rows:
             span = pl.ds(r * 512, 512)
             s = jnp.dot(qs[span, :], kt, preferred_element_type=jnp.float32)
             w = jnp.exp2(s)
@@ -208,15 +236,14 @@
                 for e in range(2):
                     hand_on(a, e, 2 * h - 1 + d).start()
 
-    for h in (1, 2, 3):
+    for h in (1, 2, 3, 4):
         first_step(h)
     for a, d in both:
         relay(a, d, 0, 0).wait_recv()
         relay(a, d, 0, 2).start()
-    first_step(4)
 
     def own(a, c):
-        attend(a * 64, a * 64 + 4)
+        attend([a * 64 + i for i in range(8)], (0, 1))
         return c
 
     lax.fori_loop(0, 2, own, 0)
@@ -228,64 +255,115 @@
                 def _():
                     relay(a, d, j, j).wait_recv()
 
-                    @pl.when(j < (5 if d == 0 else 4))
+                    @pl.when(j < 4)
                     def _():
                         relay(a, d, j, j + 2).start()
-                    if d == 1:
-                        @pl.when(j == 5)
-                        def _():
-                            relay(a, d, j, j + 1).start()
-            attend(place(a, 0, j), place(a, 1, j))
+
+                    @pl.when(j == 4 + d)
+                    def _():
+                        last(a, d, 0).start()
+                        last(a, d, 1).start()
+            attend([place(a, d, j) + i for d in range(2) for i in range(4)], (0, 1))
         return c
 
-    lax.fori_loop(0, 7, step, 0)
+    lax.fori_loop(0, 6, step, 0)
+
+    def final_slots(i):
+        return [place(a, d, 6) + 2 * i + q for a, d in both for q in range(2)]
+
+    for a, d in both:
+        last(a, d, 0).wait_recv()
+    attend(final_slots(0), (0, 1))
+    for a, d in both:
+        last(a, d, 1).wait_recv()
+
+    def project_out(r):
+        for h in range(Q_PER_KV):
+            span = slice(r * 512 + h * HALF, r * 512 + (h + 1) * HALF)
+            total = jnp.sum(lsum[span, :], axis=-1, keepdims=True)
+            att[r, :, h * HEAD_DIM:(h + 1) * HEAD_DIM] = (acc[span, :] / total).astype(jnp.bfloat16)
+        mixed = jnp.dot(att[r], wo[...], preferred_element_type=jnp.float32)
+        partial[4 * r:4 * r + 4] = mixed.reshape(4, ROWS, mixed.shape[1])
+        for i in (2 * r, 2 * r + 1):
+            to_twin[i] = partial[2 * i + 1 - core].astype(jnp.bfloat16)
+            pair(i).start()
+
+    def pair(i):
+        return pltpu.make_async_remote_copy(
+            src_ref=to_twin.at[i], dst_ref=from_twin.at[i], send_sem=ds_sem.at[i], recv_sem=dr_sem.at[i],
+            device_id=twin, device_id_type=MESH)
+
+    def along(i):
+        return pltpu.make_async_remote_copy(
+            src_ref=summed.at[i], dst_ref=arrived.at[column], send_sem=os_sem.at[i],
+            recv_sem=or_sem.at[column], device_id={"sp": sp, "tp": 2 * i + core}, device_id_type=MESH)
+
+    def arrival(source):
+        return pltpu.make_async_remote_copy(
+            src_ref=summed.at[0], dst_ref=arrived.at[source], send_sem=os_sem.at[0],
+            recv_sem=or_sem.at[source], device_id=twin, device_id_type=MESH)
+
+    def add_pair(i):
+        pair(i).wait_recv()
+        both_cores = partial[2 * i + core] + from_twin[i].astype(jnp.float32)
+        partial[2 * i + core] = both_cores
+        summed[i] = both_cores.astype(jnp.bfloat16)
+
+        @pl.when(column != i)
+        def _():
+            along(i).start()
 
     loads[4].wait()
-    for h in range(Q_PER_KV):
-        span = slice(h * BLOCK, (h + 1) * BLOCK)
-        total = jnp.sum(lsum[span, :], axis=-1, keepdims=True)
-        att[:, h * HEAD_DIM:(h + 1) * HEAD_DIM] = (acc[span, :] / total).astype(jnp.bfloat16)
-    mixed = jnp.dot(att[...], wo[...], preferred_element_type=jnp.float32)
-    part[...] = mixed.astype(jnp.bfloat16).reshape(part.shape)
-
-    def ocopy(k):
-        return pltpu.make_async_remote_copy(
-            src_ref=part.at[lax.rem(tp + k + 1, N_TP)], dst_ref=rs.at[k], send_sem=os_sem.at[k],
-            recv_sem=or_sem.at[k], device_id=peers[k], device_id_type=MESH)
-
-    for k in range(N_TP - 1):
-        ocopy(k).start()
-
-    for k in range(N_TP - 1):
-        xcopy(k).wait_send()
+    attend(final_slots(1), (0,))
+    project_out(0)
+    attend(final_slots(1), (1,))
+    add_pair(0)
+    add_pair(1)
+    project_out(1)
+
+    for i in range(2 * N_X - 1):
+        xcopy(i).wait_send()
     for a, d in both:
         for h in range(1, 5 - d):
             hop(a, h, d).wait_send()
-        for j in range(7):
+        for j in range(6):
             relay(a, d, 0, j).wait_send()
-
-    total = part[tp].astype(jnp.float32)
-    for k in range(N_TP - 1):
-        ocopy(k).wait_recv()
-        total = total + rs[k].astype(jnp.float32)
+        for i in range(2):
+            last(a, d, i).wait_send()
+
+    add_pair(2)
+    add_pair(3)
+    total = partial[tp]
+    for k in range(1, N_X):
+        source = lax.rem(column + N_X - k, N_X)
+        arrival(source).wait_recv()
+        total = total + arrived[source].astype(jnp.float32)
     out[...] = total.astype(jnp.bfloat16)
-    for k in range(N_TP - 1):
-        ocopy(k).wait_send()
+    for i in range(N_X):
+        pair(i).wait_send()
+
+        @pl.when(column != i)
+        def _():
+            along(i).wait_send()
 
 
 def on_device(tokens, valid_len, norm_gain, w_query, w_key, w_value, q_gain, k_gain, w_out):
     rows, cols = rope_constants()
     width = tokens.shape[1]
     vmem = pl.BlockSpec(memory_space=pltpu.VMEM)
-    anywhere = pl.BlockSpec(memory_space=pl.ANY)
+    anywhere = pl.BlockSpec(memory_space=pltpu.HBM)
     dma = pltpu.SemaphoreType.DMA
     call = pl.pallas_call(
         kernel,
         out_shape=jax.ShapeDtypeStruct(tokens.shape, jnp.bfloat16),
-        in_specs=[vmem, pl.BlockSpec(memory_space=pltpu.SMEM), vmem, anywhere, anywhere, anywhere,
-                  vmem, vmem, anywhere, anywhere, vmem],
+        in_specs=[anywhere, pl.BlockSpec(memory_space=pltpu.SMEM)] + [anywhere] * 9,
         out_specs=vmem,
         scratch_shapes=[
+            pltpu.VMEM(tokens.shape, jnp.bfloat16),
+            pltpu.VMEM((1, width), jnp.float32),
+            pltpu.VMEM((1, HEAD_DIM), jnp.float32),
+            pltpu.VMEM((1, HEAD_DIM), jnp.float32),
+            pltpu.VMEM(cols.shape, jnp.float32),
             pltpu.VMEM((N_TP, ROWS, width), jnp.bfloat16),
             pltpu.VMEM(w_query.shape, jnp.bfloat16),
             pltpu.VMEM(w_key.shape, jnp.bfloat16),
@@ -299,14 +377,17 @@
             pltpu.VMEM((128, 8, HALF), jnp.float32),
             pltpu.VMEM((Q_PER_KV * BLOCK, HEAD_DIM), jnp.float32),
             pltpu.VMEM((Q_PER_KV * BLOCK, HEAD_DIM), jnp.float32),
-            pltpu.VMEM((BLOCK, Q_PER_KV * HEAD_DIM), jnp.bfloat16),
-            pltpu.VMEM((N_TP, ROWS, width), jnp.bfloat16),
-            pltpu.VMEM((N_TP - 1, ROWS, width), jnp.bfloat16),
-            dma((5,)), dma((7,)), dma((7,)), dma((2, 2, 4)), dma((2, 2, 4)), dma((2, 2, 7)), dma((2, 2, 7)),
-            dma((7,)), dma((7,)),
+            pltpu.VMEM((2, HALF, Q_PER_KV * HEAD_DIM), jnp.bfloat16),
+            pltpu.VMEM((N_TP, ROWS, width), jnp.float32),
+            pltpu.VMEM((N_X, ROWS, width), jnp.bfloat16),
+            pltpu.VMEM((N_X, ROWS, width), jnp.bfloat16),
+            pltpu.VMEM((N_X, ROWS, width), jnp.bfloat16),
+            pltpu.VMEM((N_X, ROWS, width), jnp.bfloat16),
+            dma((10,)), dma((7,)), dma((7,)), dma((2, 2, 4)), dma((2, 2, 4)), dma((2, 2, 8)), dma((2, 2, 8)),
+            dma((N_X,)), dma((N_X,)), dma((N_X,)), dma((N_X,)),
         ],
         compiler_params=pltpu.CompilerParams(
-            collective_id=0, has_side_effects=True, vmem_limit_bytes=48 * 2 ** 20),
+            collective_id=0, has_side_effects=True, vmem_limit_bytes=67043328),
         name="fused_attention",
     )
     return call(tokens, valid_len, norm_gain.reshape(1, -1), w_query, w_key, w_value,

time: 94.8 us -> 82.6 us (0.87)
  local copies, waits for them, and re-layouts: 8.26 us -> 1.47 us
  Pallas kernels: 84.6 us -> 79.9 us
    unnamed x21 -> x1, local copies, waits for them, and re-layouts: 8.26 us -> 1.47 us
    pallas_call x1, Pallas kernels: 84.6 us -> 79.9 us  [on_device(): call(tokens, valid_len, norm_gain.reshape(1, -1), w_query, w_key, w_value...]
where the time goes in v2:
time: 82.6 us; the launch traced here: 82.1 us
  Pallas kernels  79.9 us (97%)
  local copies, waits for them, and re-layouts  1.47 us (2%)
    pallas_call x1, Pallas kernels, on_device(): call(tokens, valid_len, norm_gain.reshape(1, -1), w_query, w_key, w_value...  79.9 us

profile of v2, /device:TPU:1, one launch (start us, length us, event | category | flops | bytes accessed | tf_op | source)
XLA Modules:
  0.0 82.1 jit_solution(15090566811493680835)
XLA Ops:
  0.7 79.9 %fused_attention.1 = bf16[32,1024]{1,0:T(8,128)(2,1)} custom-call(bf16[32,1024]{1,0:T(8,128)(2,1)} %tok_hbm.1, s32[1]{0:T(128)S(6)} %copy.13.valid, f32[1,1024]{1,0:T(1,128)} %bitcast.3, bf16[1024,512]{1,0:T(8,128)(2,1)} %wq_hbm.1, bf16[1024,128]{1,0:T(8,128)(2,1)} %wk_hbm.1, bf16[1024,128]{1,0:T(8,128)(2,1)} %wv_hbm.1, f32[1,128]{1,0:T(1,128)} %bitcast.4, ...), custom_call_target="tpu_custom_call" | custom-call | tf_op jit(solution)/shard_map/fused_attention/pallas_call | solution.py:393
  80.6 1.5 %copy.14 = bf16[32,1024]{1,0:T(8,128)(2,1)} copy(bf16[32,1024]{1,0:T(8,128)(2,1)} %fused_attention.1) | data formatting | bytes 131072

commit v3 on v2

v3 whole, which is shorter than its diff:
```python
import functools
import math

import jax
import jax.numpy as jnp
import numpy as np
from jax import lax
from jax.experimental import pallas as pl
from jax.experimental.pallas import tpu as pltpu
from jax.sharding import PartitionSpec as P

HEAD_DIM = 128
Q_PER_KV = 4
GRID_W = 64
RING = 8
N_TP = 8
N_X = 4
ROWS = 32
BLOCK = 256
HALF = 128
EPS = 1e-06
MESH = pl.DeviceIdType.MESH
STAY = (0, 2, -2, 4)
MOVE = (1, -1, 3, -3)
SOURCE = (0, -1, -2, -3, 1, 2, 3, 4)
Q_SCALE = HEAD_DIM ** -0.5 * math.log2(math.e)


def rope_constants():
    freq = np.float32(10000.0) ** (-(np.arange(32, dtype=np.float32) * 2.0) / 64)
    freq = freq.astype(np.float32)
    sign = np.concatenate([-np.ones(32), np.ones(32)]).astype(np.float32)

    def table(count):
        angle = (np.arange(count, dtype=np.float32)[:, None] * freq[None, :]).astype(np.float64)
        angle = np.concatenate([angle, angle], axis=1)
        return np.cos(angle).astype(np.float32), np.sin(angle).astype(np.float32) * sign

    row_cos, row_sin = table(256)
    col_cos, col_sin = table(64)
    rows = np.zeros((64, 8, 128), np.float32)
    rows[:, 0:4, 0:64] = row_cos.reshape(64, 4, 64)
    rows[:, 4:8, 0:64] = row_sin.reshape(64, 4, 64)
    cols = np.zeros((2, 64, 128), np.float32)
    cols[0, :, 64:] = col_cos
    cols[1, :, 64:] = col_sin
    return rows, cols


def kernel(tok_hbm, valid, ngain_hbm, wq_hbm, wk_hbm, wv_hbm, qgain_hbm, kgain_hbm, wo_hbm, rowtab_hbm, coltab_hbm,
           out, tok, ngain, qgain, kgain, coltab, x, wq, wk, wv, wo, rowtab, cosv, sinv, mine, kv, qs, q, mask, acc, lsum, o_out, o_in, l_out, l_in, den, att, partial, to_twin, from_twin, summed, arrived,
           w_sem, xs_sem, xr_sem, s1_sem, r1_sem, s2_sem, r2_sem,
           st_sem, rt_sem, qs_sem, qr_sem, gs_sem, gr_sem, ds_sem, dr_sem, os_sem, or_sem):
    sp = lax.axis_index("sp")
    tp = lax.axis_index("tp")
    z = sp // RING
    y = sp % RING

    def wrap(a):
        return lax.rem(a + 2 * RING, RING)

    core = lax.rem(tp, 2)
    column = tp // 2
    other = tp + 1 - 2 * core
    twin = {"sp": sp, "tp": other}
    peers = [{"sp": sp, "tp": lax.rem(tp + 2 * k, N_TP)} for k in range(1, N_X)]
    moves = (core != lax.rem(y, 2), core != lax.rem(z, 2))
    moved = [m.astype(jnp.int32) for m in moves]

    def at(part_id, first, second, where):
        dz, dy = (second, first) if part_id == 0 else (first, second)
        return {"sp": wrap(z + dz) * RING + wrap(y + dy), "tp": where}

    ring = [[at(a, 0, step, tp) for step in (1, -1)] for a in range(2)]
    partner = [at(0, 1 - 2 * lax.rem(y, 2), 0, other), at(1, 1 - 2 * lax.rem(z, 2), 0, other)]

    def shift(flag, k):
        return MOVE[k] * flag + STAY[k] * (1 - flag)

    landing = [[at(a, shift(moved[a], k), 0, other * moved[a] + tp * (1 - moved[a])) for k in range(4)]
               for a in range(2)]

    loads = [
        pltpu.make_async_copy(wk_hbm, wk, w_sem.at[0]),
        pltpu.make_async_copy(wv_hbm, wv, w_sem.at[1]),
        pltpu.make_async_copy(rowtab_hbm.at[sp], rowtab, w_sem.at[2]),
        pltpu.make_async_copy(wq_hbm, wq, w_sem.at[3]),
        pltpu.make_async_copy(wo_hbm, wo, w_sem.at[4]),
        pltpu.make_async_copy(coltab_hbm, coltab, w_sem.at[5]),
        pltpu.make_async_copy(qgain_hbm, qgain, w_sem.at[6]),
        pltpu.make_async_copy(kgain_hbm, kgain, w_sem.at[7]),
    ]
    early = [
        pltpu.make_async_copy(tok_hbm, tok, w_sem.at[8]),
        pltpu.make_async_copy(ngain_hbm, ngain, w_sem.at[9]),
    ]
    for load in early:
        load.start()
    for load in loads:
        load.start()

    barrier = pltpu.get_barrier_semaphore()
    everyone = peers + [twin] + ring[0] + ring[1] + landing[0][1:] + landing[1][1:]
    for peer in everyone:
        pl.semaphore_signal(barrier, inc=1, device_id=peer, device_id_type=MESH)
    for a in range(2):
        @pl.when(moves[a])
        def _():
            pl.semaphore_signal(barrier, inc=1, device_id=landing[a][0], device_id_type=MESH)

    for load in early:
        load.wait()
    scaled = tok[...].astype(jnp.float32)
    inv = lax.rsqrt(jnp.mean(scaled * scaled, axis=-1, keepdims=True) + EPS)
    x[tp] = (scaled * inv * ngain[...]).astype(jnp.bfloat16)
    acc[...] = jnp.zeros_like(acc)
    lsum[...] = jnp.zeros_like(lsum)

    pl.semaphore_wait(barrier, len(everyone) + moved[0] + moved[1])

    def xcopy(i):
        slot = tp if i < N_X else lax.rem(tp + 2 * N_TP - 2 * (i - N_X + 1), N_TP)
        return pltpu.make_async_remote_copy(
            src_ref=x.at[slot], dst_ref=x.at[slot], send_sem=xs_sem.at[i], recv_sem=xr_sem.at[i],
            device_id=peers[i - 1] if 0 < i < N_X else twin, device_id_type=MESH)

    for i in (2, 1, 3, 0):
        xcopy(i).start()

    for i in (2, 5, 6, 7):
        loads[i].wait()
    for r in range(4):
        cosv[r * 64:(r + 1) * 64, :] = rowtab[r:r + 1, :] + coltab[0]
        sinv[r * 64:(r + 1) * 64, :] = rowtab[4 + r:5 + r, :] + coltab[1]

    limit = valid[0]
    lane = lax.broadcasted_iota(jnp.int32, (1, HALF), 1)

    def mask_row(slot, block, half):
        pos = block * BLOCK + half * HALF + lane
        mask[slot] = jnp.broadcast_to((pos < limit).astype(jnp.float32), (8, HALF))

    for a in range(2):
        for side in range(2):
            flag = moved[a] if side == 0 else 1 - moved[a]
            for e in range(8):
                for k in range(4):
                    place = at(a, -shift(flag, k), SOURCE[e], tp)
                    mask_row(a * 64 + side * 32 + e * 4 + k, place["sp"], a)

    loads[0].wait()
    loads[1].wait()
    for k in (1, 3, 2):
        xcopy(k).wait_recv()
        xcopy(k + N_X - 1).start()
    for i in (0, 4, 6, 5):
        xcopy(i).wait_recv()

    everything = x[...].reshape(BLOCK, x.shape[2])
    cosine = cosv[...]
    sine = sinv[...]
    in_first = (lax.broadcasted_iota(jnp.int32, (BLOCK, HEAD_DIM), 1) % 64) < 32

    def turn(projected, gain, factor):
        v = projected.astype(jnp.bfloat16).astype(jnp.float32)
        u = v * lax.rsqrt(jnp.mean(v * v, axis=-1, keepdims=True) + EPS) * gain
        moved = jnp.where(in_first, pltpu.roll(u, 96, 1), pltpu.roll(u, 32, 1))
        return (u * cosine + moved * sine) * factor

    keys = turn(jnp.dot(everything, wk[...], preferred_element_type=jnp.float32), kgain[...], 1.0)
    rows = sp * BLOCK + lax.broadcasted_iota(jnp.int32, (BLOCK, HEAD_DIM), 0)
    vals = jnp.dot(everything, wv[...], preferred_element_type=jnp.float32)
    vals = jnp.where(rows < limit, vals, 0.0).astype(jnp.bfloat16)
    for a in range(2):
        piece = slice(a * HALF, (a + 1) * HALF)
        mine[a, 0:HALF, :] = keys[piece, :].T.astype(jnp.bfloat16)
        mine[a, HALF:, :] = vals[piece, :]

    def spread(a, k):
        return pltpu.make_async_remote_copy(
            src_ref=mine.at[a], dst_ref=kv.at[a * 64 + k], send_sem=s1_sem.at[a, k], recv_sem=r1_sem.at[a, k],
            device_id=landing[a][k], device_id_type=MESH)

    def slot(a, side, e, p):
        return a * 64 + side * 32 + e * 4 + 2 * p

    def hop(a, d, p, e_from, e_to, i):
        return pltpu.make_async_remote_copy(
            src_ref=kv.at[pl.ds(slot(a, 0, e_from, p), 2)], dst_ref=kv.at[pl.ds(slot(a, 0, e_to, p), 2)],
            send_sem=s2_sem.at[a, d, i], recv_sem=r2_sem.at[a, d, i],
            device_id=ring[a][d], device_id_type=MESH)

    def share(a, e, p):
        return pltpu.make_async_remote_copy(
            src_ref=kv.at[pl.ds(slot(a, 0, e, p), 2)], dst_ref=kv.at[pl.ds(slot(a, 1, e, p), 2)],
            send_sem=st_sem.at[a, e, p], recv_sem=rt_sem.at[a, e, p],
            device_id=twin, device_id_type=MESH)

    for k in (1, 0, 2, 3):
        for a in range(2):
            if k == 0:
                @pl.when(moves[a])
                def _():
                    spread(a, 0).start()

                @pl.when(jnp.logical_not(moves[a]))
                def _():
                    kv[a * 64] = mine[a]
            else:
                spread(a, k).start()

    loads[3].wait()
    for h in range(Q_PER_KV):
        query = jnp.dot(everything, wq[:, h * HEAD_DIM:(h + 1) * HEAD_DIM], preferred_element_type=jnp.float32)
        query = turn(query, qgain[...], Q_SCALE).astype(jnp.bfloat16)
        for r in range(2):
            qs[r * 512 + h * HALF:r * 512 + (h + 1) * HALF, :] = query[r * HALF:(r + 1) * HALF, :]

    def swap_query(a):
        return pltpu.make_async_remote_copy(
            src_ref=qs, dst_ref=q.at[a], send_sem=qs_sem.at[a], recv_sem=qr_sem.at[a],
            device_id=partner[a], device_id_type=MESH)

    for a in range(2):
        @pl.when(moves[a])
        def _():
            swap_query(a).start()

        @pl.when(jnp.logical_not(moves[a]))
        def _():
            q[a] = qs[...]

    def attend(a, slots, rows):
        kt = jnp.concatenate([kv[s, 0:HALF, :] for s in slots], axis=1)
        v = jnp.concatenate([kv[s, HALF:, :] for s in slots], axis=0)
        marks = [mask[s, 0:1, :] for s in slots]
        for r in rows:
            span = pl.ds(r * 512, 512)
            s = jnp.dot(q[a, span, :], kt, preferred_element_type=jnp.float32)
            w = jnp.exp2(s)
            acc[a, span, :] += jnp.dot(w.astype(jnp.bfloat16), v, preferred_element_type=jnp.float32)
            t = w[:, 0:HALF] * marks[0]
            for i in range(1, 8):
                t = t + w[:, i * HALF:(i + 1) * HALF] * marks[i]
            lsum[a, span, :] += t

    for p in range(2):
        for a in range(2):
            if p == 0:
                @pl.when(moves[a])
                def _():
                    spread(a, 0).wait_recv()
            else:
                spread(a, 2).wait_recv()
            spread(a, 2 * p + 1).wait_recv()
            for d in range(2):
                hop(a, d, p, 0, 3 * d + 1, p).start()
            share(a, 0, p).start()

    for a in range(2):
        @pl.when(moves[a])
        def _():
            swap_query(a).wait_recv()

    def own(a, c):
        for p in range(2):
            share(a, 0, p).wait_recv()
        attend(a, [slot(a, side, 0, 0) + i for side in range(2) for i in range(4)], (0, 1))
        return c

    lax.fori_loop(0, 2, own, 0)

    def receive(i):
        e, p = i // 2 + 1, lax.rem(i, 2)
        for a in range(2):
            for d in range(2):
                hop(a, d, p, 0, 3 * d + e, i).wait_recv()

                @pl.when(i < 4)
                def _():
                    hop(a, d, p, 3 * d + e, 3 * d + e + 1, i + 2).start()

                @pl.when(i == 4 + d)
                def _():
                    hop(a, d, d, 3 * d + 3, 7, 6).start()
                share(a, 3 * d + e, p).start()

    def receive_last(d):
        for a in range(2):
            hop(a, d, d, 0, 7, 6).wait_recv()
            share(a, 7, d).start()

    def use(a, i):
        e, p = i // 2 + 1, lax.rem(i, 2)
        for d in range(2):
            share(a, 3 * d + e, p).wait_recv()
        attend(a, [slot(a, side, 3 * d + e, p) + n for side in range(2) for d in range(2) for n in range(2)], (0, 1))

    receive(jnp.int32(0))

    def stage(i, c):
        use(0, i)

        @pl.when(i < 5)
        def _():
            receive(i + 1)

        @pl.when(i == 5)
        def _():
            receive_last(0)
        use(1, i)
        return c

    lax.fori_loop(0, 6, stage, 0)
    receive_last(1)

    def give_back(a, r):
        return (
            pltpu.make_async_remote_copy(
                src_ref=o_out.at[a, r], dst_ref=o_in.at[a, r], send_sem=gs_sem.at[a, r, 0],
                recv_sem=gr_sem.at[a, r, 0], device_id=partner[a], device_id_type=MESH),
            pltpu.make_async_remote_copy(
                src_ref=l_out.at[a, r], dst_ref=l_in.at[a, r], send_sem=gs_sem.at[a, r, 1],
                recv_sem=gr_sem.at[a, r, 1], device_id=partner[a], device_id_type=MESH),
        )

    ones = jnp.ones((8, HALF), jnp.float32)

    def finish(a, r):
        span = slice(r * 512, (r + 1) * 512)
        l_out[a, r] = lax.dot_general(ones, lsum[a, span, :], (((1,), (1,)), ((), ())),
                                      precision=lax.Precision.HIGHEST, preferred_element_type=jnp.float32)

        @pl.when(moves[a])
        def _():
            o_out[a, r] = acc[a, span, :].astype(jnp.bfloat16)
            for copy in give_back(a, r):
                copy.start()

    def gather_back(r):
        span = slice(r * 512, (r + 1) * 512)
        for a in range(2):
            @pl.when(moves[a])
            def _():
                for copy in give_back(a, r):
                    copy.wait_recv()
                acc[a, span, :] = o_in[a, r].astype(jnp.float32)
                den[a, r] = l_in[a, r]

            @pl.when(jnp.logical_not(moves[a]))
            def _():
                den[a, r] = l_out[a, r]

    def final_slots(a):
        return [slot(a, side, 7, 0) + i for side in range(2) for i in range(4)]

    def project_out(r):
        totals = (den[0, r] + den[1, r]).T
        for h in range(Q_PER_KV):
            span = slice(r * 512 + h * HALF, r * 512 + (h + 1) * HALF)
            rows_of = slice(h * HALF, (h + 1) * HALF)
            att[r, :, h * HEAD_DIM:(h + 1) * HEAD_DIM] = (
                (acc[0, span, :] + acc[1, span, :]) / totals[rows_of, 0:1]).astype(jnp.bfloat16)
        mixed = jnp.dot(att[r], wo[...], preferred_element_type=jnp.float32)
        partial[4 * r:4 * r + 4] = mixed.reshape(4, ROWS, mixed.shape[1])
        for i in (2 * r, 2 * r + 1):
            to_twin[i] = partial[2 * i + 1 - core].astype(jnp.bfloat16)
            pair(i).start()

    def pair(i):
        return pltpu.make_async_remote_copy(
            src_ref=to_twin.at[i], dst_ref=from_twin.at[i], send_sem=ds_sem.at[i], recv_sem=dr_sem.at[i],
            device_id=twin, device_id_type=MESH)

    def along(i):
        return pltpu.make_async_remote_copy(
            src_ref=summed.at[i], dst_ref=arrived.at[column], send_sem=os_sem.at[i],
            recv_sem=or_sem.at[column], device_id={"sp": sp, "tp": 2 * i + core}, device_id_type=MESH)

    def arrival(source):
        return pltpu.make_async_remote_copy(
            src_ref=summed.at[0], dst_ref=arrived.at[source], send_sem=os_sem.at[0],
            recv_sem=or_sem.at[source], device_id=twin, device_id_type=MESH)

    def add_pair(i):
        pair(i).wait_recv()
        both_cores = partial[2 * i + core] + from_twin[i].astype(jnp.float32)
        partial[2 * i + core] = both_cores
        summed[i] = both_cores.astype(jnp.bfloat16)

        @pl.when(column != i)
        def _():
            along(i).start()

    for a in range(2):
        for p in range(2):
            share(a, 7, p).wait_recv()
    for r in range(2):
        for a in range(2):
            attend(a, final_slots(a), (r,))
            finish(a, r)

    loads[4].wait()
    for i in range(2 * N_X - 1):
        xcopy(i).wait_send()
    for a in range(2):
        for k in range(1, 4):
            spread(a, k).wait_send()

        @pl.when(moves[a])
        def _():
            spread(a, 0).wait_send()
            swap_query(a).wait_send()
        for d in range(2):
            for i in range(7):
                hop(a, d, 0, 0, 1, i).wait_send()
        for e in range(8):
            for p in range(2):
                share(a, e, p).wait_send()

    for r in range(2):
        gather_back(r)
        project_out(r)
        add_pair(2 * r)
        add_pair(2 * r + 1)
    total = partial[tp]
    for k in range(1, N_X):
        source = lax.rem(column + N_X - k, N_X)
        arrival(source).wait_recv()
        total = total + arrived[source].astype(jnp.float32)
    out[...] = total.astype(jnp.bfloat16)
    for a in range(2):
        @pl.when(moves[a])
        def _():
            for r in range(2):
                for copy in give_back(a, r):
                    copy.wait_send()
    for i in range(N_X):
        pair(i).wait_send()

        @pl.when(column != i)
        def _():
            along(i).wait_send()


def on_device(tokens, valid_len, norm_gain, w_query, w_key, w_value, q_gain, k_gain, w_out):
    rows, cols = rope_constants()
    width = tokens.shape[1]
    vmem = pl.BlockSpec(memory_space=pltpu.VMEM)
    anywhere = pl.BlockSpec(memory_space=pltpu.HBM)
    dma = pltpu.SemaphoreType.DMA
    call = pl.pallas_call(
        kernel,
        out_shape=jax.ShapeDtypeStruct(tokens.shape, jnp.bfloat16),
        in_specs=[anywhere, pl.BlockSpec(memory_space=pltpu.SMEM)] + [anywhere] * 9,
        out_specs=vmem,
        scratch_shapes=[
            pltpu.VMEM(tokens.shape, jnp.bfloat16),
            pltpu.VMEM((1, width), jnp.float32),
            pltpu.VMEM((1, HEAD_DIM), jnp.float32),
            pltpu.VMEM((1, HEAD_DIM), jnp.float32),
            pltpu.VMEM(cols.shape, jnp.float32),
            pltpu.VMEM((N_TP, ROWS, width), jnp.bfloat16),
            pltpu.VMEM(w_query.shape, jnp.bfloat16),
            pltpu.VMEM(w_key.shape, jnp.bfloat16),
            pltpu.VMEM(w_value.shape, jnp.bfloat16),
            pltpu.VMEM(w_out.shape, jnp.bfloat16),
            pltpu.VMEM((8, HEAD_DIM), jnp.float32),
            pltpu.VMEM((BLOCK, HEAD_DIM), jnp.float32),
            pltpu.VMEM((BLOCK, HEAD_DIM), jnp.float32),
            pltpu.VMEM((2, 2 * HALF, HEAD_DIM), jnp.bfloat16),
            pltpu.VMEM((128, 2 * HALF, HEAD_DIM), jnp.bfloat16),
            pltpu.VMEM((Q_PER_KV * BLOCK, HEAD_DIM), jnp.bfloat16),
            pltpu.VMEM((2, Q_PER_KV * BLOCK, HEAD_DIM), jnp.bfloat16),
            pltpu.VMEM((128, 8, HALF), jnp.float32),
            pltpu.VMEM((2, Q_PER_KV * BLOCK, HEAD_DIM), jnp.float32),
            pltpu.VMEM((2, Q_PER_KV * BLOCK, HEAD_DIM), jnp.float32),
            pltpu.VMEM((2, 2, 512, HEAD_DIM), jnp.bfloat16),
            pltpu.VMEM((2, 2, 512, HEAD_DIM), jnp.bfloat16),
            pltpu.VMEM((2, 2, 8, 512), jnp.float32),
            pltpu.VMEM((2, 2, 8, 512), jnp.float32),
            pltpu.VMEM((2, 2, 8, 512), jnp.float32),
            pltpu.VMEM((2, HALF, Q_PER_KV * HEAD_DIM), jnp.bfloat16),
            pltpu.VMEM((N_TP, ROWS, width), jnp.float32),
            pltpu.VMEM((N_X, ROWS, width), jnp.bfloat16),
            pltpu.VMEM((N_X, ROWS, width), jnp.bfloat16),
            pltpu.VMEM((N_X, ROWS, width), jnp.bfloat16),
            pltpu.VMEM((N_X, ROWS, width), jnp.bfloat16),
            dma((10,)), dma((7,)), dma((7,)), dma((2, 4)), dma((2, 4)), dma((2, 2, 7)), dma((2, 2, 7)),
            dma((2, 8, 2)), dma((2, 8, 2)), dma((2,)), dma((2,)), dma((2, 2, 2)), dma((2, 2, 2)),
            dma((N_X,)), dma((N_X,)), dma((N_X,)), dma((N_X,)),
        ],
        compiler_params=pltpu.CompilerParams(
            collective_id=0, has_side_effects=True, vmem_limit_bytes=67043328),
        name="fused_attention",
    )
    return call(tokens, valid_len, norm_gain.reshape(1, -1), w_query, w_key, w_value,
                q_gain.reshape(1, -1), k_gain.reshape(1, -1), w_out, jnp.asarray(rows), jnp.asarray(cols))


def solution(mesh):
    return jax.shard_map(
        on_device,
        mesh=mesh,
        in_specs=(
            P(("sp", "tp"), None),
            P(),
            P(),
            P(None, "tp"),
            P(None, "tp"),
            P(None, "tp"),
            P(),
            P(),
            P("tp", None),
        ),
        out_specs=P(("sp", "tp"), None),
        check_vma=False,
    )
```

time: 82.6 us -> 72.9 us (0.88)
  Pallas kernels: 79.9 us -> 70.1 us
    pallas_call x1, Pallas kernels: 79.9 us -> 70.1 us  [on_device(): call(tokens, valid_len, norm_gain.reshape(1, -1), w_query, w_key, w_value...]
where the time goes in v3:
time: 72.9 us; the launch traced here: 72.2 us
  Pallas kernels  70.1 us (96%)
  local copies, waits for them, and re-layouts  1.47 us (2%)
    pallas_call x1, Pallas kernels, on_device(): call(tokens, valid_len, norm_gain.reshape(1, -1), w_query, w_key, w_value...  70.1 us
    unnamed x1, local copies, waits for them, and re-layouts  1.47 us

profile of v3, /device:TPU:1, one launch (start us, length us, event | category | flops | bytes accessed | tf_op | source)
XLA Modules:
  0.0 72.2 jit_solution(2000926104399009604)
XLA Ops:
  0.7 70.1 %fused_attention.1 = bf16[32,1024]{1,0:T(8,128)(2,1)} custom-call(bf16[32,1024]{1,0:T(8,128)(2,1)} %tok_hbm.1, s32[1]{0:T(128)S(6)} %copy.13.valid, f32[1,1024]{1,0:T(1,128)} %bitcast.3, bf16[1024,512]{1,0:T(8,128)(2,1)} %wq_hbm.1, bf16[1024,128]{1,0:T(8,128)(2,1)} %wk_hbm.1, bf16[1024,128]{1,0:T(8,128)(2,1)} %wv_hbm.1, f32[1,128]{1,0:T(1,128)} %bitcast.4, ...), custom_call_target="tpu_custom_call" | custom-call | tf_op jit(solution)/shard_map/fused_attention/pallas_call | solution.py:497
  70.8 1.5 %copy.14 = bf16[32,1024]{1,0:T(8,128)(2,1)} copy(bf16[32,1024]{1,0:T(8,128)(2,1)} %fused_attention.1) | data formatting | bytes 131072

commit v4 on v3

--- a/solution.py
+++ b/solution.py
@@ -47,8 +47,8 @@
     return rows, cols
 
 
-def kernel(tok_hbm, valid, ngain_hbm, wq_hbm, wk_hbm, wv_hbm, qgain_hbm, kgain_hbm, wo_hbm, rowtab_hbm, coltab_hbm,
-           out, tok, ngain, qgain, kgain, coltab, x, wq, wk, wv, wo, rowtab, cosv, sinv, mine, kv, qs, q, mask, acc, lsum, o_out, o_in, l_out, l_in, den, att, partial, to_twin, from_twin, summed, arrived,
+def kernel(tok_hbm, valid_hbm, ngain_hbm, wq_hbm, wk_hbm, wv_hbm, qgain_hbm, kgain_hbm, wo_hbm, rowtab_hbm, coltab_hbm,
+           out, tok, valid, ngain, qgain, kgain, coltab, x, wq, wk, wv, wo, rowtab, cosv, sinv, mine, kv, qs, q, mask, acc, lsum, o_out, o_in, l_out, l_in, den, att, partial, to_twin, from_twin, summed, arrived,
            w_sem, xs_sem, xr_sem, s1_sem, r1_sem, s2_sem, r2_sem,
            st_sem, rt_sem, qs_sem, qr_sem, gs_sem, gr_sem, ds_sem, dr_sem, os_sem, or_sem):
     sp = lax.axis_index("sp")
@@ -77,7 +77,11 @@
     def shift(flag, k):
         return MOVE[k] * flag + STAY[k] * (1 - flag)
 
-    landing = [[at(a, shift(moved[a], k), 0, other * moved[a] + tp * (1 - moved[a])) for k in range(4)]
+    def choose(a, if_moved, if_not):
+        return if_moved * moved[a] + if_not * (1 - moved[a])
+
+    two_on = [[at(a, step, 0, tp) for step in (2, -2)] for a in range(2)]
+    landing = [[at(a, shift(moved[a], k), 0, choose(a, other, tp)) for k in range(3)]
                for a in range(2)]
 
     loads = [
@@ -93,6 +97,7 @@
     early = [
         pltpu.make_async_copy(tok_hbm, tok, w_sem.at[8]),
         pltpu.make_async_copy(ngain_hbm, ngain, w_sem.at[9]),
+        pltpu.make_async_copy(valid_hbm, valid, w_sem.at[10]),
     ]
     for load in early:
         load.start()
@@ -100,13 +105,14 @@
         load.start()
 
     barrier = pltpu.get_barrier_semaphore()
-    everyone = peers + [twin] + ring[0] + ring[1] + landing[0][1:] + landing[1][1:]
+    everyone = peers + [twin] + ring[0] + ring[1] + two_on[0] + two_on[1]
     for peer in everyone:
         pl.semaphore_signal(barrier, inc=1, device_id=peer, device_id_type=MESH)
     for a in range(2):
         @pl.when(moves[a])
         def _():
-            pl.semaphore_signal(barrier, inc=1, device_id=landing[a][0], device_id_type=MESH)
+            for k in range(2):
+                pl.semaphore_signal(barrier, inc=1, device_id=landing[a][k], device_id_type=MESH)
 
     for load in early:
         load.wait()
@@ -116,12 +122,16 @@
     acc[...] = jnp.zeros_like(acc)
     lsum[...] = jnp.zeros_like(lsum)
 
-    pl.semaphore_wait(barrier, len(everyone) + moved[0] + moved[1])
+    pl.semaphore_wait(barrier, len(everyone) + 2 * moved[0] + 2 * moved[1])
+
+    def together(ref, send, recv):
+        return pltpu.make_async_remote_copy(
+            src_ref=ref, dst_ref=ref, send_sem=send, recv_sem=recv, device_id=twin, device_id_type=MESH)
 
     def xcopy(i):
         slot = tp if i < N_X else lax.rem(tp + 2 * N_TP - 2 * (i - N_X + 1), N_TP)
         return pltpu.make_async_remote_copy(
-            src_ref=x.at[slot], dst_ref=x.at[slot], send_sem=xs_sem.at[i], recv_sem=xr_sem.at[i],
+            src_ref=x.at[slot], dst_ref=x.at[slot], send_sem=xs_sem.at[0], recv_sem=xr_sem.at[i],
             device_id=peers[i - 1] if 0 < i < N_X else twin, device_id_type=MESH)
 
     for i in (2, 1, 3, 0):
@@ -178,8 +188,20 @@
 
     def spread(a, k):
         return pltpu.make_async_remote_copy(
-            src_ref=mine.at[a], dst_ref=kv.at[a * 64 + k], send_sem=s1_sem.at[a, k], recv_sem=r1_sem.at[a, k],
+            src_ref=mine.at[a], dst_ref=kv.at[a * 64 + k], send_sem=s1_sem.at[a], recv_sem=r1_sem.at[a, k],
             device_id=landing[a][k], device_id_type=MESH)
+
+    def pass_up(a):
+        return pltpu.make_async_remote_copy(
+            src_ref=kv.at[a * 64], dst_ref=kv.at[a * 64 + 2], send_sem=s1_sem.at[a], recv_sem=r1_sem.at[a, 2],
+            device_id=two_on[a][0], device_id_type=MESH)
+
+    def pass_on(a):
+        odd = lax.rem((y if a == 0 else z) // 2, 2)
+        upwards = odd * (1 - moved[a])
+        return pltpu.make_async_remote_copy(
+            src_ref=kv.at[a * 64 + choose(a, 1, 2 - odd)], dst_ref=kv.at[a * 64 + 3], send_sem=s1_sem.at[a],
+            recv_sem=r1_sem.at[a, 3], device_id=at(a, 4 * upwards - 2, 0, tp), device_id_type=MESH)
 
     def slot(a, side, e, p):
         return a * 64 + side * 32 + e * 4 + 2 * p
@@ -187,34 +209,34 @@
     def hop(a, d, p, e_from, e_to, i):
         return pltpu.make_async_remote_copy(
             src_ref=kv.at[pl.ds(slot(a, 0, e_from, p), 2)], dst_ref=kv.at[pl.ds(slot(a, 0, e_to, p), 2)],
-            send_sem=s2_sem.at[a, d, i], recv_sem=r2_sem.at[a, d, i],
+            send_sem=s2_sem.at[0], recv_sem=r2_sem.at[a, i + d if isinstance(i, int) and i == 6 else i],
             device_id=ring[a][d], device_id_type=MESH)
 
-    def share(a, e, p):
+    def share(a, e, p, i):
         return pltpu.make_async_remote_copy(
             src_ref=kv.at[pl.ds(slot(a, 0, e, p), 2)], dst_ref=kv.at[pl.ds(slot(a, 1, e, p), 2)],
-            send_sem=st_sem.at[a, e, p], recv_sem=rt_sem.at[a, e, p],
+            send_sem=st_sem.at[0], recv_sem=rt_sem.at[a, i],
             device_id=twin, device_id_type=MESH)
 
-    for k in (1, 0, 2, 3):
-        for a in range(2):
-            if k == 0:
-                @pl.when(moves[a])
-                def _():
-                    spread(a, 0).start()
-
-                @pl.when(jnp.logical_not(moves[a]))
-                def _():
-                    kv[a * 64] = mine[a]
-            else:
-                spread(a, k).start()
+    for a in range(2):
+        spread(a, 1).start()
+
+        @pl.when(moves[a])
+        def _():
+            spread(a, 0).start()
+
+        @pl.when(jnp.logical_not(moves[a]))
+        def _():
+            spread(a, 2).start()
+            kv[a * 64] = mine[a]
 
     loads[3].wait()
     for h in range(Q_PER_KV):
         query = jnp.dot(everything, wq[:, h * HEAD_DIM:(h + 1) * HEAD_DIM], preferred_element_type=jnp.float32)
         query = turn(query, qgain[...], Q_SCALE).astype(jnp.bfloat16)
+        query = query.reshape(N_TP, 2, ROWS // 2, HEAD_DIM)
         for r in range(2):
-            qs[r * 512 + h * HALF:r * 512 + (h + 1) * HALF, :] = query[r * HALF:(r + 1) * HALF, :]
+            qs[r * 512 + h * HALF:r * 512 + (h + 1) * HALF, :] = query[:, r].reshape(HALF, HEAD_DIM)
 
     def swap_query(a):
         return pltpu.make_async_remote_copy(
@@ -240,42 +262,52 @@
             w = jnp.exp2(s)
             acc[a, span, :] += jnp.dot(w.astype(jnp.bfloat16), v, preferred_element_type=jnp.float32)
             t = w[:, 0:HALF] * marks[0]
-            for i in range(1, 8):
+            for i in range(1, len(slots)):
                 t = t + w[:, i * HALF:(i + 1) * HALF] * marks[i]
             lsum[a, span, :] += t
 
-    for p in range(2):
-        for a in range(2):
-            if p == 0:
-                @pl.when(moves[a])
-                def _():
-                    spread(a, 0).wait_recv()
-            else:
-                spread(a, 2).wait_recv()
-            spread(a, 2 * p + 1).wait_recv()
-            for d in range(2):
-                hop(a, d, p, 0, 3 * d + 1, p).start()
-            share(a, 0, p).start()
+    def hand_on(a, p):
+        for d in range(2):
+            hop(a, d, p, 0, 3 * d + 1, p).start()
+        share(a, 0, p, p).start()
+
+    for a in range(2):
+        @pl.when(moves[a])
+        def _():
+            spread(a, 0).wait_recv()
+            pass_up(a).start()
+        spread(a, 1).wait_recv()
+
+        @pl.when(jnp.logical_not(moves[a]))
+        def _():
+            spread(a, 2).wait_recv()
+        pass_on(a).start()
+    for a in range(2):
+        hand_on(a, 0)
 
     for a in range(2):
         @pl.when(moves[a])
         def _():
             swap_query(a).wait_recv()
 
-    def own(a, c):
-        for p in range(2):
-            share(a, 0, p).wait_recv()
-        attend(a, [slot(a, side, 0, 0) + i for side in range(2) for i in range(4)], (0, 1))
-        return c
-
-    lax.fori_loop(0, 2, own, 0)
+    def own(a, p):
+        share(a, 0, p, p).wait_recv()
+        attend(a, [slot(a, side, 0, p) + i for side in range(2) for i in range(2)], (0, 1))
+
+    for a in range(2):
+        own(a, 0)
+    for a in range(2):
+        @pl.when(moves[a])
+        def _():
+            pass_up(a).wait_recv()
+        pass_on(a).wait_recv()
+        hand_on(a, 1)
 
     def receive(i):
         e, p = i // 2 + 1, lax.rem(i, 2)
         for a in range(2):
+            together(kv.at[pl.ds(a * 64, 4)], s2_sem.at[0], r2_sem.at[a, i]).wait_recv()
             for d in range(2):
-                hop(a, d, p, 0, 3 * d + e, i).wait_recv()
-
                 @pl.when(i < 4)
                 def _():
                     hop(a, d, p, 3 * d + e, 3 * d + e + 1, i + 2).start()
@@ -283,20 +315,21 @@
                 @pl.when(i == 4 + d)
                 def _():
                     hop(a, d, d, 3 * d + 3, 7, 6).start()
-                share(a, 3 * d + e, p).start()
+                share(a, 3 * d + e, p, i + 2).start()
 
     def receive_last(d):
         for a in range(2):
             hop(a, d, d, 0, 7, 6).wait_recv()
-            share(a, 7, d).start()
+            share(a, 7, d, 8 + d).start()
 
     def use(a, i):
         e, p = i // 2 + 1, lax.rem(i, 2)
-        for d in range(2):
-            share(a, 3 * d + e, p).wait_recv()
+        together(kv.at[pl.ds(a * 64, 4)], st_sem.at[0], rt_sem.at[a, i + 2]).wait_recv()
         attend(a, [slot(a, side, 3 * d + e, p) + n for side in range(2) for d in range(2) for n in range(2)], (0, 1))
 
+    own(0, 1)
     receive(jnp.int32(0))
+    own(1, 1)
 
     def stage(i, c):
         use(0, i)
@@ -312,24 +345,35 @@
         return c
 
     lax.fori_loop(0, 6, stage, 0)
+
+    def final_slots(a, p):
+        share(a, 7, p, 8 + p).wait_recv()
+        return [slot(a, side, 7, p) + i for side in range(2) for i in range(2)]
+
+    attend(0, final_slots(0, 0), (0, 1))
     receive_last(1)
+    attend(1, final_slots(1, 0), (0, 1))
 
     def give_back(a, r):
         return (
             pltpu.make_async_remote_copy(
-                src_ref=o_out.at[a, r], dst_ref=o_in.at[a, r], send_sem=gs_sem.at[a, r, 0],
+                src_ref=o_out.at[a, r], dst_ref=o_in.at[a, r], send_sem=gs_sem.at[a, 0],
                 recv_sem=gr_sem.at[a, r, 0], device_id=partner[a], device_id_type=MESH),
             pltpu.make_async_remote_copy(
-                src_ref=l_out.at[a, r], dst_ref=l_in.at[a, r], send_sem=gs_sem.at[a, r, 1],
+                src_ref=l_out.at[a, r], dst_ref=l_in.at[a, r], send_sem=gs_sem.at[a, 1],
                 recv_sem=gr_sem.at[a, r, 1], device_id=partner[a], device_id_type=MESH),
         )
 
-    ones = jnp.ones((8, HALF), jnp.float32)
+    ones = jnp.ones((8, HALF), jnp.bfloat16)
 
     def finish(a, r):
         span = slice(r * 512, (r + 1) * 512)
-        l_out[a, r] = lax.dot_general(ones, lsum[a, span, :], (((1,), (1,)), ((), ())),
-                                      precision=lax.Precision.HIGHEST, preferred_element_type=jnp.float32)
+        sums = lsum[a, span, :]
+        high = sums.astype(jnp.bfloat16)
+        low = (sums - high.astype(jnp.float32)).astype(jnp.bfloat16)
+        across = (((1,), (1,)), ((), ()))
+        l_out[a, r] = (lax.dot_general(ones, high, across, preferred_element_type=jnp.float32)
+                       + lax.dot_general(ones, low, across, preferred_element_type=jnp.float32))
 
         @pl.when(moves[a])
         def _():
@@ -351,9 +395,6 @@
             def _():
                 den[a, r] = l_out[a, r]
 
-    def final_slots(a):
-        return [slot(a, side, 7, 0) + i for side in range(2) for i in range(4)]
-
     def project_out(r):
         totals = (den[0, r] + den[1, r]).T
         for h in range(Q_PER_KV):
@@ -362,85 +403,75 @@
             att[r, :, h * HEAD_DIM:(h + 1) * HEAD_DIM] = (
                 (acc[0, span, :] + acc[1, span, :]) / totals[rows_of, 0:1]).astype(jnp.bfloat16)
         mixed = jnp.dot(att[r], wo[...], preferred_element_type=jnp.float32)
-        partial[4 * r:4 * r + 4] = mixed.reshape(4, ROWS, mixed.shape[1])
-        for i in (2 * r, 2 * r + 1):
-            to_twin[i] = partial[2 * i + 1 - core].astype(jnp.bfloat16)
-            pair(i).start()
-
-    def pair(i):
-        return pltpu.make_async_remote_copy(
-            src_ref=to_twin.at[i], dst_ref=from_twin.at[i], send_sem=ds_sem.at[i], recv_sem=dr_sem.at[i],
+        part_rows = slice(r * ROWS // 2, (r + 1) * ROWS // 2)
+        partial[:, part_rows, :] = mixed.reshape(N_TP, ROWS // 2, mixed.shape[1])
+        for i in range(N_X):
+            to_twin[r, i] = partial[2 * i + 1 - core, part_rows, :].astype(jnp.bfloat16)
+        pair(r).start()
+
+    def pair(r):
+        return pltpu.make_async_remote_copy(
+            src_ref=to_twin.at[r], dst_ref=from_twin.at[r], send_sem=ds_sem.at[r], recv_sem=dr_sem.at[r],
             device_id=twin, device_id_type=MESH)
 
-    def along(i):
-        return pltpu.make_async_remote_copy(
-            src_ref=summed.at[i], dst_ref=arrived.at[column], send_sem=os_sem.at[i],
-            recv_sem=or_sem.at[column], device_id={"sp": sp, "tp": 2 * i + core}, device_id_type=MESH)
-
-    def arrival(source):
-        return pltpu.make_async_remote_copy(
-            src_ref=summed.at[0], dst_ref=arrived.at[source], send_sem=os_sem.at[0],
-            recv_sem=or_sem.at[source], device_id=twin, device_id_type=MESH)
-
-    def add_pair(i):
-        pair(i).wait_recv()
-        both_cores = partial[2 * i + core] + from_twin[i].astype(jnp.float32)
-        partial[2 * i + core] = both_cores
-        summed[i] = both_cores.astype(jnp.bfloat16)
-
-        @pl.when(column != i)
-        def _():
-            along(i).start()
-
-    for a in range(2):
-        for p in range(2):
-            share(a, 7, p).wait_recv()
+    def along(r, i):
+        return pltpu.make_async_remote_copy(
+            src_ref=summed.at[r, i], dst_ref=arrived.at[r, column], send_sem=os_sem.at[r],
+            recv_sem=or_sem.at[r], device_id={"sp": sp, "tp": 2 * i + core}, device_id_type=MESH)
+
+    def add_pair(r):
+        pair(r).wait_recv()
+        part_rows = slice(r * ROWS // 2, (r + 1) * ROWS // 2)
+        for i in range(N_X):
+            both_cores = partial[2 * i + core, part_rows, :] + from_twin[r, i].astype(jnp.float32)
+            partial[2 * i + core, part_rows, :] = both_cores
+            summed[r, i] = both_cores.astype(jnp.bfloat16)
+
+            @pl.when(column != i)
+            def _():
+                along(r, i).start()
+
+    slots = [final_slots(a, 1) for a in range(2)]
     for r in range(2):
         for a in range(2):
-            attend(a, final_slots(a), (r,))
+            attend(a, slots[a], (r,))
             finish(a, r)
 
     loads[4].wait()
-    for i in range(2 * N_X - 1):
-        xcopy(i).wait_send()
-    for a in range(2):
-        for k in range(1, 4):
-            spread(a, k).wait_send()
-
-        @pl.when(moves[a])
-        def _():
-            spread(a, 0).wait_send()
+    together(x.at[pl.ds(0, 2 * N_X - 1)], xs_sem.at[0], xr_sem.at[0]).wait_send()
+    for a in range(2):
+        @pl.when(moves[a])
+        def _():
+            together(kv.at[pl.ds(0, 4)], s1_sem.at[a], r1_sem.at[a, 0]).wait_send()
             swap_query(a).wait_send()
-        for d in range(2):
-            for i in range(7):
-                hop(a, d, 0, 0, 1, i).wait_send()
-        for e in range(8):
-            for p in range(2):
-                share(a, e, p).wait_send()
-
+
+        @pl.when(jnp.logical_not(moves[a]))
+        def _():
+            together(kv.at[pl.ds(0, 3)], s1_sem.at[a], r1_sem.at[a, 0]).wait_send()
+    together(kv.at[pl.ds(0, 56)], s2_sem.at[0], r2_sem.at[0, 0]).wait_send()
+    together(kv.at[pl.ds(0, 64)], st_sem.at[0], rt_sem.at[0, 0]).wait_send()
+
+    gather_back(0)
+    project_out(0)
+    gather_back(1)
+    add_pair(0)
+    project_out(1)
+    add_pair(1)
     for r in range(2):
-        gather_back(r)
-        project_out(r)
-        add_pair(2 * r)
-        add_pair(2 * r + 1)
-    total = partial[tp]
-    for k in range(1, N_X):
-        source = lax.rem(column + N_X - k, N_X)
-        arrival(source).wait_recv()
-        total = total + arrived[source].astype(jnp.float32)
-    out[...] = total.astype(jnp.bfloat16)
-    for a in range(2):
-        @pl.when(moves[a])
-        def _():
-            for r in range(2):
-                for copy in give_back(a, r):
-                    copy.wait_send()
-    for i in range(N_X):
-        pair(i).wait_send()
-
-        @pl.when(column != i)
-        def _():
-            along(i).wait_send()
+        part_rows = slice(r * ROWS // 2, (r + 1) * ROWS // 2)
+        total = partial[tp, part_rows, :]
+        together(arrived.at[r, pl.ds(0, N_X - 1)], os_sem.at[r], or_sem.at[r]).wait_recv()
+        for k in range(1, N_X):
+            total = total + arrived[r, lax.rem(column + N_X - k, N_X)].astype(jnp.float32)
+        out[part_rows, :] = total.astype(jnp.bfloat16)
+    for a in range(2):
+        @pl.when(moves[a])
+        def _():
+            together(o_out.at[a], gs_sem.at[a, 0], gr_sem.at[a, 0, 0]).wait_send()
+            together(l_out.at[a], gs_sem.at[a, 1], gr_sem.at[a, 0, 1]).wait_send()
+    for r in range(2):
+        pair(r).wait_send()
+        together(summed.at[r, pl.ds(0, N_X - 1)], os_sem.at[r], or_sem.at[r]).wait_send()
 
 
 def on_device(tokens, valid_len, norm_gain, w_query, w_key, w_value, q_gain, k_gain, w_out):
@@ -452,10 +483,11 @@
     call = pl.pallas_call(
         kernel,
         out_shape=jax.ShapeDtypeStruct(tokens.shape, jnp.bfloat16),
-        in_specs=[anywhere, pl.BlockSpec(memory_space=pltpu.SMEM)] + [anywhere] * 9,
+        in_specs=[anywhere] * 11,
         out_specs=vmem,
         scratch_shapes=[
             pltpu.VMEM(tokens.shape, jnp.bfloat16),
+            pltpu.SMEM((1,), jnp.int32),
             pltpu.VMEM((1, width), jnp.float32),
             pltpu.VMEM((1, HEAD_DIM), jnp.float32),
             pltpu.VMEM((1, HEAD_DIM), jnp.float32),
@@ -482,13 +514,13 @@
             pltpu.VMEM((2, 2, 8, 512), jnp.float32),
             pltpu.VMEM((2, HALF, Q_PER_KV * HEAD_DIM), jnp.bfloat16),
             pltpu.VMEM((N_TP, ROWS, width), jnp.float32),
-            pltpu.VMEM((N_X, ROWS, width), jnp.bfloat16),
-            pltpu.VMEM((N_X, ROWS, width), jnp.bfloat16),
-            pltpu.VMEM((N_X, ROWS, width), jnp.bfloat16),
-            pltpu.VMEM((N_X, ROWS, width), jnp.bfloat16),
-            dma((10,)), dma((7,)), dma((7,)), dma((2, 4)), dma((2, 4)), dma((2, 2, 7)), dma((2, 2, 7)),
-            dma((2, 8, 2)), dma((2, 8, 2)), dma((2,)), dma((2,)), dma((2, 2, 2)), dma((2, 2, 2)),
-            dma((N_X,)), dma((N_X,)), dma((N_X,)), dma((N_X,)),
+            pltpu.VMEM((2, N_X, ROWS // 2, width), jnp.bfloat16),
+            pltpu.VMEM((2, N_X, ROWS // 2, width), jnp.bfloat16),
+            pltpu.VMEM((2, N_X, ROWS // 2, width), jnp.bfloat16),
+            pltpu.VMEM((2, N_X, ROWS // 2, width), jnp.bfloat16),
+            dma((11,)), dma((1,)), dma((7,)), dma((2,)), dma((2, 4)), dma((1,)), dma((2, 8)),
+            dma((1,)), dma((2, 10)), dma((2,)), dma((2,)), dma((2, 2)), dma((2, 2, 2)),
+            dma((2,)), dma((2,)), dma((2,)), dma((2,)),
         ],
         compiler_params=pltpu.CompilerParams(
             collective_id=0, has_side_effects=True, vmem_limit_bytes=67043328),

time: 72.9 us -> 70 us (0.960)
  Pallas kernels: 70.1 us -> 67.6 us
    pallas_call x1, Pallas kernels: 70.1 us -> 67.6 us  [on_device(): call(tokens, valid_len, norm_gain.reshape(1, -1), w_query, w_key, w_value...]
where the time goes in v4:
time: 70 us; the launch traced here: 69.8 us
  Pallas kernels  67.6 us (97%)
  local copies, waits for them, and re-layouts  1.47 us (2%)
    pallas_call x1, Pallas kernels, on_device(): call(tokens, valid_len, norm_gain.reshape(1, -1), w_query, w_key, w_value...  67.6 us
    unnamed x1, local copies, waits for them, and re-layouts  1.47 us

profile of v4, /device:TPU:1, one launch (start us, length us, event | category | flops | bytes accessed | tf_op | source)
XLA Modules:
  0.0 69.8 jit_solution(16615053535619941825)
XLA Ops:
  0.7 67.6 %fused_attention.1 = bf16[32,1024]{1,0:T(8,128)(2,1)} custom-call(bf16[32,1024]{1,0:T(8,128)(2,1)} %tok_hbm.1, s32[1]{0:T(128)S(6)} %copy.13.valid_hbm, f32[1,1024]{1,0:T(1,128)} %bitcast.3, bf16[1024,512]{1,0:T(8,128)(2,1)} %wq_hbm.1, bf16[1024,128]{1,0:T(8,128)(2,1)} %wk_hbm.1, bf16[1024,128]{1,0:T(8,128)(2,1)} %wv_hbm.1, f32[1,128]{1,0:T(1,128)} %bitcast.4, ...), custom_call_target="tpu_custom_call" | custom-call | tf_op jit(solution)/shard_map/fused_attention/pallas_call | solution.py:529
  68.3 1.5 %copy.14 = bf16[32,1024]{1,0:T(8,128)(2,1)} copy(bf16[32,1024]{1,0:T(8,128)(2,1)} %fused_attention.1) | data formatting | bytes 131072

commit v5 on v4

--- a/solution.py
+++ b/solution.py
@@ -523,11 +523,12 @@
             dma((2,)), dma((2,)), dma((2,)), dma((2,)),
         ],
         compiler_params=pltpu.CompilerParams(
-            collective_id=0, has_side_effects=True, vmem_limit_bytes=67043328),
+            collective_id=0, has_side_effects=True, vmem_limit_bytes=48 * 2 ** 20),
         name="fused_attention",
     )
-    return call(tokens, valid_len, norm_gain.reshape(1, -1), w_query, w_key, w_value,
+    operands = (tokens, valid_len, norm_gain.reshape(1, -1), w_query, w_key, w_value,
                 q_gain.reshape(1, -1), k_gain.reshape(1, -1), w_out, jnp.asarray(rows), jnp.asarray(cols))
+    return call(*[o if o is valid_len else pltpu.with_memory_space_constraint(o, pltpu.HBM) for o in operands])
 
 
 def solution(mesh):

time: 70 us -> 68.4 us (0.977)
  local copies, waits for them, and re-layouts: 1.47 us -> 0.63 us
    unnamed x1, local copies, waits for them, and re-layouts: 1.47 us -> 0.63 us
where the time goes in v5:
time: 68.4 us; the launch traced here: 68.3 us
  Pallas kernels  67 us (98%)
    pallas_call x1, Pallas kernels, on_device(): call(*[o if o is valid_len else pltpu.with_memory_space_constraint(o, plt...  67 us

profile of v5, /device:TPU:1, one launch (start us, length us, event | category | flops | bytes accessed | tf_op | source)
XLA Modules:
  0.0 68.3 jit_solution(18159463047939338822)
XLA Ops:
  0.7 67.0 %fused_attention.1 = bf16[32,1024]{1,0:T(8,128)(2,1)S(1)} custom-call(bf16[32,1024]{1,0:T(8,128)(2,1)} %tok_hbm.1, s32[1]{0:T(128)S(6)} %copy.13.valid_hbm, f32[1,1024]{1,0:T(1,128)} %bitcast.3, bf16[1024,512]{1,0:T(8,128)(2,1)} %wq_hbm.1, bf16[1024,128]{1,0:T(8,128)(2,1)} %wk_hbm.1, bf16[1024,128]{1,0:T(8,128)(2,1)} %wv_hbm.1, f32[1,128]{1,0:T(1,128)} %bitcast.4, ...), custom_call_target="tpu_custom_call" | custom-call | tf_op jit(solution)/shard_map/fused_attention/pallas_call | solution.py:531
  67.7 0.6 copy.14

commit v6 on v5

--- a/solution.py
+++ b/solution.py
@@ -186,22 +186,24 @@
         mine[a, 0:HALF, :] = keys[piece, :].T.astype(jnp.bfloat16)
         mine[a, HALF:, :] = vals[piece, :]
 
-    def spread(a, k):
-        return pltpu.make_async_remote_copy(
-            src_ref=mine.at[a], dst_ref=kv.at[a * 64 + k], send_sem=s1_sem.at[a], recv_sem=r1_sem.at[a, k],
+    def spread(a, k, h):
+        return pltpu.make_async_remote_copy(
+            src_ref=mine.at[a, pl.ds(h * HALF, HALF)], dst_ref=kv.at[a * 64 + k, pl.ds(h * HALF, HALF)],
+            send_sem=s1_sem.at[a], recv_sem=r1_sem.at[a, k, h],
             device_id=landing[a][k], device_id_type=MESH)
 
-    def pass_up(a):
-        return pltpu.make_async_remote_copy(
-            src_ref=kv.at[a * 64], dst_ref=kv.at[a * 64 + 2], send_sem=s1_sem.at[a], recv_sem=r1_sem.at[a, 2],
+    def pass_up(a, h):
+        return pltpu.make_async_remote_copy(
+            src_ref=kv.at[a * 64, pl.ds(h * HALF, HALF)], dst_ref=kv.at[a * 64 + 2, pl.ds(h * HALF, HALF)],
+            send_sem=s1_sem.at[a], recv_sem=r1_sem.at[a, 2, h],
             device_id=two_on[a][0], device_id_type=MESH)
 
-    def pass_on(a):
+    def pass_on(a, h):
         odd = lax.rem((y if a == 0 else z) // 2, 2)
         upwards = odd * (1 - moved[a])
         return pltpu.make_async_remote_copy(
-            src_ref=kv.at[a * 64 + choose(a, 1, 2 - odd)], dst_ref=kv.at[a * 64 + 3], send_sem=s1_sem.at[a],
-            recv_sem=r1_sem.at[a, 3], device_id=at(a, 4 * upwards - 2, 0, tp), device_id_type=MESH)
+            src_ref=kv.at[a * 64 + choose(a, 1, 2 - odd), pl.ds(h * HALF, HALF)],
+            dst_ref=kv.at[a * 64 + 3, pl.ds(h * HALF, HALF)], send_sem=s1_sem.at[a], recv_sem=r1_sem.at[a, 3, h], device_id=at(a, 4 * upwards - 2, 0, tp), device_id_type=MESH)
 
     def slot(a, side, e, p):
         return a * 64 + side * 32 + e * 4 + 2 * p
@@ -218,17 +220,18 @@
             send_sem=st_sem.at[0], recv_sem=rt_sem.at[a, i],
             device_id=twin, device_id_type=MESH)
 
-    for a in range(2):
-        spread(a, 1).start()
-
-        @pl.when(moves[a])
-        def _():
-            spread(a, 0).start()
-
-        @pl.when(jnp.logical_not(moves[a]))
-        def _():
-            spread(a, 2).start()
-            kv[a * 64] = mine[a]
+    for h in range(2):
+        for a in range(2):
+            spread(a, 1, h).start()
+
+            @pl.when(moves[a])
+            def _():
+                spread(a, 0, h).start()
+
+            @pl.when(jnp.logical_not(moves[a]))
+            def _():
+                spread(a, 2, h).start()
+                kv[a * 64, h * HALF:(h + 1) * HALF, :] = mine[a, h * HALF:(h + 1) * HALF, :]
 
     loads[3].wait()
     for h in range(Q_PER_KV):
@@ -271,17 +274,18 @@
             hop(a, d, p, 0, 3 * d + 1, p).start()
         share(a, 0, p, p).start()
 
-    for a in range(2):
-        @pl.when(moves[a])
-        def _():
-            spread(a, 0).wait_recv()
-            pass_up(a).start()
-        spread(a, 1).wait_recv()
-
-        @pl.when(jnp.logical_not(moves[a]))
-        def _():
-            spread(a, 2).wait_recv()
-        pass_on(a).start()
+    for h in range(2):
+        for a in range(2):
+            @pl.when(moves[a])
+            def _():
+                spread(a, 0, h).wait_recv()
+                pass_up(a, h).start()
+            spread(a, 1, h).wait_recv()
+
+            @pl.when(jnp.logical_not(moves[a]))
+            def _():
+                spread(a, 2, h).wait_recv()
+            pass_on(a, h).start()
     for a in range(2):
         hand_on(a, 0)
 
@@ -299,8 +303,10 @@
     for a in range(2):
         @pl.when(moves[a])
         def _():
-            pass_up(a).wait_recv()
-        pass_on(a).wait_recv()
+            for h in range(2):
+                pass_up(a, h).wait_recv()
+        for h in range(2):
+            pass_on(a, h).wait_recv()
         hand_on(a, 1)
 
     def receive(i):
@@ -368,6 +374,11 @@
 
     def finish(a, r):
         span = slice(r * 512, (r + 1) * 512)
+        @pl.when(moves[a])
+        def _():
+            o_out[a, r] = acc[a, span, :].astype(jnp.bfloat16)
+            give_back(a, r)[0].start()
+
         sums = lsum[a, span, :]
         high = sums.astype(jnp.bfloat16)
         low = (sums - high.astype(jnp.float32)).astype(jnp.bfloat16)
@@ -377,9 +388,7 @@
 
         @pl.when(moves[a])
         def _():
-            o_out[a, r] = acc[a, span, :].astype(jnp.bfloat16)
-            for copy in give_back(a, r):
-                copy.start()
+            give_back(a, r)[1].start()
 
     def gather_back(r):
         span = slice(r * 512, (r + 1) * 512)
@@ -435,6 +444,7 @@
     for r in range(2):
         for a in range(2):
             attend(a, slots[a], (r,))
+        for a in range(2):
             finish(a, r)
 
     loads[4].wait()
@@ -442,12 +452,12 @@
     for a in range(2):
         @pl.when(moves[a])
         def _():
-            together(kv.at[pl.ds(0, 4)], s1_sem.at[a], r1_sem.at[a, 0]).wait_send()
+            together(kv.at[pl.ds(0, 4)], s1_sem.at[a], r1_sem.at[a, 0, 0]).wait_send()
             swap_query(a).wait_send()
 
         @pl.when(jnp.logical_not(moves[a]))
         def _():
-            together(kv.at[pl.ds(0, 3)], s1_sem.at[a], r1_sem.at[a, 0]).wait_send()
+            together(kv.at[pl.ds(0, 3)], s1_sem.at[a], r1_sem.at[a, 0, 0]).wait_send()
     together(kv.at[pl.ds(0, 56)], s2_sem.at[0], r2_sem.at[0, 0]).wait_send()
     together(kv.at[pl.ds(0, 64)], st_sem.at[0], rt_sem.at[0, 0]).wait_send()
 
@@ -518,7 +528,7 @@
             pltpu.VMEM((2, N_X, ROWS // 2, width), jnp.bfloat16),
             pltpu.VMEM((2, N_X, ROWS // 2, width), jnp.bfloat16),
             pltpu.VMEM((2, N_X, ROWS // 2, width), jnp.bfloat16),
-            dma((11,)), dma((1,)), dma((7,)), dma((2,)), dma((2, 4)), dma((1,)), dma((2, 8)),
+            dma((11,)), dma((1,)), dma((7,)), dma((2,)), dma((2, 4, 2)), dma((1,)), dma((2, 8)),
             dma((1,)), dma((2, 10)), dma((2,)), dma((2,)), dma((2, 2)), dma((2, 2, 2)),
             dma((2,)), dma((2,)), dma((2,)), dma((2,)),
         ],

time: 68.4 us -> 68 us (level)
  no operation moved by 1% of the time
where the time goes in v6:
time: 68 us; the launch traced here: 67.8 us
  Pallas kernels  66.5 us (98%)
    pallas_call x1, Pallas kernels, on_device(): call(*[o if o is valid_len else pltpu.with_memory_space_constraint(o, plt...  66.5 us

profile of v6, /device:TPU:1, one launch (start us, length us, event | category | flops | bytes accessed | tf_op | source)
XLA Modules:
  0.0 67.8 jit_solution(6461181168738216963)
XLA Ops:
  0.7 66.5 %fused_attention.1 = bf16[32,1024]{1,0:T(8,128)(2,1)S(1)} custom-call(bf16[32,1024]{1,0:T(8,128)(2,1)} %tok_hbm.1, s32[1]{0:T(128)S(6)} %copy.13.valid_hbm, f32[1,1024]{1,0:T(1,128)} %bitcast.3, bf16[1024,512]{1,0:T(8,128)(2,1)} %wq_hbm.1, bf16[1024,128]{1,0:T(8,128)(2,1)} %wk_hbm.1, bf16[1024,128]{1,0:T(8,128)(2,1)} %wv_hbm.1, f32[1,128]{1,0:T(1,128)} %bitcast.4, ...), custom_call_target="tpu_custom_call" | custom-call | tf_op jit(solution)/shard_map/fused_attention/pallas_call | solution.py:541
  67.2 0.6 copy.14
